TPU v7x, 32 devices: a whole 2x2x4 slice. The times are simulated.
32 devices in a mesh: sp: 16 (over z, y, x), tp: 2 (over core).
Axes of the slice: x: 2, y: 2, z: 4, core: 2. Of those that a mesh axis runs over, the one named last changes fastest.
Arguments:
- resid: bfloat16 [6144, 2048], P('sp', 'tp'), may hold values from -40 to 40
- query_one: bfloat16 [6144, 1024], P('sp', 'tp'), may hold values from -64 to 64
- key_one: bfloat16 [6144, 1024], P('sp', 'tp'), may hold values from -64 to 64
- query_two: bfloat16 [6144, 1024], P('sp', 'tp'), may hold values from -64 to 64
- key_two: bfloat16 [6144, 1024], P('sp', 'tp'), may hold values from -64 to 64
- values: bfloat16 [6144, 2048], P('sp', 'tp'), may hold values from -6 to 6
- mix_lambda: float32 [8], P('tp'), may hold values from 0.3 to 0.8
- segments: int32 [6144], P('sp'), may hold values from 0 to 7, never falling along the last dimension, each value on 1 to 1536 neighbouring positions
- head_gain: float32 [256], replicated, may hold values from 0.1 to 1.9
- out_weight: bfloat16 [2048, 2048], P(None, 'tp'), may hold values from -0.125 to 0.125
- mixer_gain: float32 [2048], P('tp'), may hold values from 0.1 to 1.9
- gate_weight: bfloat16 [2048, 6144], P('sp', 'tp'), may hold values from -0.125 to 0.125
- up_weight: bfloat16 [2048, 6144], P('sp', 'tp'), may hold values from -0.125 to 0.125
- down_weight: bfloat16 [6144, 2048], P('tp', 'sp'), may hold values from -0.078125 to 0.078125
Outputs:
- layer_out: bfloat16 [6144, 2048], P('sp', 'tp')
Inputs may be any that keep to these rules, and one draw needn't show every extreme that they name: `segments`: numbers never fall along the sequence; each document has at most 1536 positions and one has exactly that many.
All inputs are finite; a program needn't handle non-finite values.
Results may differ from a plain program's by a relative error of at most 0.012.
Values may be sent and summed in bfloat16 or wider, within the bound.
A program may use at most 128 MiB of HBM per device.

v0:
```python
import jax
import jax.numpy as jnp
from jax import lax
from jax.sharding import PartitionSpec as P

HD = 128
VD = 256
REACH = 4


def shifted(value, axis, by):
    length = lax.axis_size(axis)
    pairs = [(i, i + by) for i in range(length) if 0 <= i + by < length]
    return lax.ppermute(value, axis, pairs)


def body(
    resid,
    query_one,
    key_one,
    query_two,
    key_two,
    values,
    mix_lambda,
    segments,
    head_gain,
    out_weight,
    mixer_gain,
    gate_weight,
    up_weight,
    down_weight,
):
    rows = query_one.shape[0]
    heads = mix_lambda.shape[0]
    position = lax.axis_index("sp")
    carried = (key_one, key_two, values, segments)
    earlier = [carried]
    for step in range(REACH):
        carried = shifted((carried[0], carried[1], carried[2], carried[3]), "sp", 1)
        earlier.insert(0, carried)
    width = (REACH + 1) * rows
    k_first = jnp.concatenate([piece[0] for piece in earlier], 0).reshape(width, heads, HD)
    k_second = jnp.concatenate([piece[1] for piece in earlier], 0).reshape(width, heads, HD)
    vals = jnp.concatenate([piece[2] for piece in earlier], 0).reshape(width, heads, VD)
    seg_key = jnp.concatenate([piece[3] for piece in earlier], 0)
    q_pos = position * rows + jnp.arange(rows, dtype=jnp.int32)
    k_pos = (position - REACH) * rows + jnp.arange(width, dtype=jnp.int32)
    allowed = (
        (seg_key[None, :] == segments[:, None])
        & (k_pos[None, :] <= q_pos[:, None])
        & (k_pos[None, :] >= 0)
    )

    def weights(query, keys):
        score = jnp.einsum(
            "qhd,khd->hqk", query.reshape(rows, heads, HD), keys, preferred_element_type=jnp.float32
        ) * HD ** (-0.5)
        score = jnp.where(allowed[None], score, -jnp.inf)
        score = score - jnp.max(score, axis=-1, keepdims=True)
        expo = jnp.exp(score)
        return (expo / jnp.sum(expo, axis=-1, keepdims=True)).astype(jnp.bfloat16)

    out_first = jnp.einsum(
        "hqk,khe->qhe", weights(query_one, k_first), vals, preferred_element_type=jnp.float32
    )
    out_second = jnp.einsum(
        "hqk,khe->qhe", weights(query_two, k_second), vals, preferred_element_type=jnp.float32
    )
    head_out = out_first - mix_lambda[None, :, None] * out_second
    meansq = jnp.mean(head_out * head_out, axis=-1, keepdims=True)
    attn_rows = (
        (head_out * lax.rsqrt(meansq + 1e-05) * head_gain)
        .reshape(rows, heads * VD)
        .astype(jnp.bfloat16)
    )
    projected = jnp.dot(
        lax.all_gather(attn_rows, "tp", axis=1, tiled=True),
        out_weight,
        preferred_element_type=jnp.float32,
    )
    mid = (resid.astype(jnp.float32) + projected).astype(jnp.bfloat16)
    midf = mid.astype(jnp.float32)
    squares = lax.psum(jnp.sum(midf * midf, axis=1), "tp")
    channels = mid.shape[1] * lax.axis_size("tp")
    normed = (midf * lax.rsqrt(squares / channels + 1e-06)[:, None] * mixer_gain).astype(
        jnp.bfloat16
    )
    whole_rows = lax.all_gather(normed, "tp", axis=1, tiled=True)
    gate = jnp.dot(
        whole_rows,
        lax.all_gather(gate_weight, "sp", axis=0, tiled=True),
        preferred_element_type=jnp.float32,
    )
    up = jnp.dot(
        whole_rows,
        lax.all_gather(up_weight, "sp", axis=0, tiled=True),
        preferred_element_type=jnp.float32,
    )
    hidden = (jax.nn.silu(gate) * up).astype(jnp.bfloat16)
    terms = jnp.dot(
        hidden,
        lax.all_gather(down_weight, "sp", axis=1, tiled=True),
        preferred_element_type=jnp.float32,
    )
    summed = lax.psum_scatter(
        terms.astype(jnp.bfloat16), "tp", scatter_dimension=1, tiled=True
    ).astype(jnp.float32)
    return (midf + summed).astype(jnp.bfloat16)


def solution(mesh):
    in_specs = (
        P("sp", "tp"),
        P("sp", "tp"),
        P("sp", "tp"),
        P("sp", "tp"),
        P("sp", "tp"),
        P("sp", "tp"),
        P("tp"),
        P("sp"),
        P(),
        P(None, "tp"),
        P("tp"),
        P("sp", "tp"),
        P("sp", "tp"),
        P("tp", "sp"),
    )
    out_specs = P("sp", "tp")
    return jax.shard_map(body, mesh=mesh, in_specs=in_specs, out_specs=out_specs, check_vma=False)
```

profile of v0, /device:TPU:16, one launch (start us, length us, event | category | flops | bytes accessed | tf_op | source)
XLA Modules:
  0.0 767.5 jit_solution(17959958012359783923)
XLA Ops:
  7.8 3.4 collective-permute-start.12
  11.2 3.4 collective-permute-start.4
  14.6 3.4 collective-permute-start
  19.2 3.4 collective-permute-start.8
  23.5 2.5 collective-permute-start.5
  26.1 3.4 collective-permute-start.13
  29.5 19.3 %collective-permute-done.5 = s32[384]{0:T(512)S(1)} collective-permute-done((s32[384]{0:T(512)S(1)}, s32[384]{0:T(512)S(1)}, u32[]{:S(2)}, u32[]{:S(2)}) %collective-permute-start.5) | collective-permute-done | bytes 1568 | tf_op jit(solution)/shard_map/ppermute | solution.py:14
  50.8 5.4 collective-permute-done.6
  58.1 5.3 collective-permute-done.7
  65.4 3.1 collective-permute-start.14
  69.2 9.9 %collective-permute-done.9 = bf16[384,512]{0,1:T(8,128)(2,1)S(1)} collective-permute-done((bf16[384,512]{0,1:T(8,128)(2,1)S(1)}, bf16[384,512]{0,1:T(8,128)(2,1)S(1)}, u32[]{:S(2)}, u32[]{:S(2)}) %collective-permute-start.9) | collective-permute-done | bytes 393248 | tf_op jit(solution)/shard_map/ppermute | solution.py:14
  81.1 6.5 collective-permute-done.14
  89.5 2.5 and_and_fusion
  98.0 6.4 collective-permute-done.15
  106.8 6.2 fusion.19
  112.9 17.4 %fusion.30 = (f32[4,384]{1,0:T(4,128)S(1)}, f32[4,384,1920]{1,2,0:T(8,128)}) fusion(f32[4,1920,384]{2,1,0:T(8,128)} %fusion.19, pred[384,1920]{0,1:T(8,128)(4,1)S(1)} %and_and_fusion), kind=kOutput, calls=%fused_computation.71 | output fusion | flops 17696640 | bytes 24336384 | tf_op jit(solution)/shard_map/sub | solution.py:59
  135.7 6.1 fusion.22
  141.8 6.3 collective-permute-done.2
  150.2 17.7 %fusion.31 = (f32[4,384]{1,0:T(4,128)S(1)}, f32[4,384,1920]{1,2,0:T(8,128)}) fusion(f32[4,1920,384]{2,1,0:T(8,128)} %fusion.22, pred[384,1920]{0,1:T(8,128)(4,1)} %copy-done.4), kind=kOutput, calls=%fused_computation.72 | output fusion | flops 17696640 | bytes 24336384 | tf_op jit(solution)/shard_map/sub | solution.py:59
  172.7 6.3 copy.20
  179.0 8.0 %fusion.9 = f32[4,256,384]{2,1,0:T(8,128)S(1)} fusion(bf16[1920,4,256]{0,2,1:T(8,128)(2,1)} %bitcast.60, f32[4,384,1920]{1,2,0:T(8,128)} %get-tuple-element.6, f32[4,384]{1,0:T(4,128)S(1)} %get-tuple-element.5), kind=kOutput, calls=%fused_computation.15 | convolution fusion | flops 1515847680 | bytes 17307648 | tf_op jit(solution)/shard_map/hqk,khe->qhe/dot_general | solution.py:66
  187.0 6.8 fusion.16
  195.2 11.5 %all-gather.6.cloned.1.call-done = bf16[384,2048]{0,1:T(8,128)(2,1)} async-done(((bf16[384,1024]{0,1:T(8,128)(2,1)}), bf16[384,2048]{0,1:T(8,128)(2,1)}) %all-gather.6.cloned.1.call-update) | async-done | bytes 1572880 | tf_op jit(solution)/shard_map/all_gather | solution.py:77
  206.7 4.6 fusion.12
  211.3 2.5 psum.7
  216.9 9.2 %all-gather.8.cloned.1.call-done = bf16[384,2048]{1,0:T(8,128)(2,1)} async-done(((bf16[384,1024]{1,0:T(8,128)(2,1)}), bf16[384,2048]{1,0:T(8,128)(2,1)}) %all-gather.8.cloned.1.call-update) | async-done | bytes 1572880 | tf_op jit(solution)/shard_map/all_gather | solution.py:88
  226.1 154.2 %all-gather.10.cloned.1.call-done = bf16[2048,3072]{1,0:T(8,128)(2,1)} async-done(((bf16[128,3072]{1,0:T(8,128)(2,1)}), bf16[2048,3072]{1,0:T(8,128)(2,1)}) %all-gather.10.cloned.1.call-update) | async-done | bytes 12582928 | tf_op jit(solution)/shard_map/all_gather | solution.py:91
  380.3 9.9 %fusion.32 = f32[384,3072]{1,0:T(8,128)} fusion(bf16[384,2048]{1,0:T(8,128)(2,1)} %all-gather.8.cloned.1.call-done, bf16[2048,3072]{1,0:T(8,128)(2,1)} %all-gather.10.cloned.1.call-done), kind=kOutput, calls=%fused_computation.73 | convolution fusion | flops 4831838208 | bytes 18874368 | tf_op jit(solution)/shard_map/dot_general | solution.py:89
  390.2 142.4 %all-gather.12.cloned.1.call-done = bf16[2048,3072]{1,0:T(8,128)(2,1)} async-done(((bf16[128,3072]{1,0:T(8,128)(2,1)}), bf16[2048,3072]{1,0:T(8,128)(2,1)}) %all-gather.12.cloned.1.call-update) | async-done | bytes 12582928 | tf_op jit(solution)/shard_map/all_gather | solution.py:96
  532.6 196.2 %all-gather.14.cloned.1.call-done = bf16[3072,2048]{1,0:T(8,128)(2,1)} async-done(((bf16[3072,128]{1,0:T(8,128)(2,1)}), bf16[3072,2048]{1,0:T(8,128)(2,1)}) %all-gather.14.cloned.1.call-update) | async-done | bytes 12582928 | tf_op jit(solution)/shard_map/all_gather | solution.py:102
  728.8 21.0 %convolution_convert_fusion = bf16[384,2048]{1,0:T(8,128)(2,1)} fusion(bf16[3072,2048]{1,0:T(8,128)(2,1)} %all-gather.14.cloned.1.call-done, f32[384,3072]{1,0:T(8,128)} %fusion.32, bf16[384,2048]{1,0:T(8,128)(2,1)S(1)} %copy-done.13, bf16[2048,3072]{1,0:T(8,128)(2,1)} %all-gather.12.cloned.1.call-done), kind=kOutput, calls=%fused_computation.20 | convolution fusion | flops 9671540736 | bytes 33030144 | tf_op jit(solution)/shard_map/dot_general | solution.py:100
  749.8 8.5 %reduce-scatter.2.cloned.1.call-done = bf16[384,1024]{1,0:T(8,128)(2,1)} async-done(((bf16[384,2048]{1,0:T(8,128)(2,1)}), bf16[384,1024]{1,0:T(8,128)(2,1)}) %reduce-scatter.2.cloned.1.call-update) | async-done | bytes 786448 | tf_op jit(solution)/shard_map/reduce_scatter | solution.py:105
  (93 shorter events, 40.9 us)
Async XLA Ops:
  6.5 100.2 %copy-start = (bf16[384,512]{1,0:T(8,128)(2,1)S(1)}, bf16[384,512]{1,0:T(8,128)(2,1)}, u32[]{:S(2)}) copy-start(bf16[384,512]{1,0:T(8,128)(2,1)} %param.17) | copy-start | bytes 1179652
  6.5 200.1 %all-gather.6.cloned.1.call-start = ((), (), s32[]{:S(2)}) async-start(), calls=%async_computation.1 | async-start | bytes 2359296 | tf_op jit(solution)/shard_map/all_gather | solution.py:77
  7.8 18.3 %collective-permute-start.12 = (bf16[384,512]{0,1:T(8,128)(2,1)S(1)}, bf16[384,512]{0,1:T(8,128)(2,1)S(1)}, u32[]{:S(2)}, u32[]{:S(2)}) collective-permute-start(bf16[384,512]{0,1:T(8,128)(2,1)S(1)} %copy.26), channel_id=1, source_target_pairs={{0,2},{2,4},{4,6},{6,8},{8,10},{10,12},{12,14},{14,16},{16,18},{18... | collective-permute-start | bytes 1179656 | tf_op jit(solution)/shard_map/ppermute | solution.py:14
  11.2 12.3 %collective-permute-start.4 = (s32[384]{0:T(512)}, s32[384]{0:T(512)S(1)}, u32[]{:S(2)}, u32[]{:S(2)}) collective-permute-start(s32[384]{0:T(512)} %param.21), channel_id=1, source_target_pairs={{0,2},{2,4},{4,6},{6,8},{8,10},{10,12},{12,14},{14,16},{16,18},{18... | collective-permute-start | bytes 4616 | tf_op jit(solution)/shard_map/ppermute | solution.py:14
  14.6 77.5 %collective-permute-start = (bf16[384,1024]{1,0:T(8,128)(2,1)}, bf16[384,1024]{1,0:T(8,128)(2,1)S(1)}, u32[]{:S(2)}, u32[]{:S(2)}) collective-permute-start(bf16[384,1024]{1,0:T(8,128)(2,1)} %param.19), channel_id=1, source_target_pairs={{0,2},{2,4},{4,6},{6,8},{8,10},{10,12},{12,14},{14,16},{16,18},{18... | collective-permute-start | bytes 2359304 | tf_op jit(solution)/shard_map/ppermute | solution.py:14
  19.2 44.2 %collective-permute-start.8 = (bf16[384,512]{0,1:T(8,128)(2,1)S(1)}, bf16[384,512]{0,1:T(8,128)(2,1)S(1)}, u32[]{:S(2)}, u32[]{:S(2)}) collective-permute-start(bf16[384,512]{0,1:T(8,128)(2,1)S(1)} %copy.21), channel_id=1, source_target_pairs={{0,2},{2,4},{4,6},{6,8},{8,10},{10,12},{12,14},{14,16},{16,18},{18... | collective-permute-start | bytes 1179656 | tf_op jit(solution)/shard_map/ppermute | solution.py:14
  23.5 25.3 %collective-permute-start.5 = (s32[384]{0:T(512)S(1)}, s32[384]{0:T(512)S(1)}, u32[]{:S(2)}, u32[]{:S(2)}) collective-permute-start(s32[384]{0:T(512)S(1)} %collective-permute-done.4), channel_id=1, source_target_pairs={{0,2},{2,4},{4,6},{6,8},{8,10},{10,12},{12,14},{14,16},{16,18},{18... | collective-permute-start | bytes 4616 | tf_op jit(solution)/shard_map/ppermute | solution.py:14
  26.1 66.0 %copy-start.8 = (bf16[384,512]{0,1:T(8,128)(2,1)}, bf16[384,512]{0,1:T(8,128)(2,1)S(1)}, u32[]{:S(2)}) copy-start(bf16[384,512]{0,1:T(8,128)(2,1)S(1)} %collective-permute-done.12) | copy-start | bytes 1179652
  26.1 39.3 %collective-permute-start.13 = (bf16[384,512]{0,1:T(8,128)(2,1)S(1)}, bf16[384,512]{0,1:T(8,128)(2,1)S(1)}, u32[]{:S(2)}, u32[]{:S(2)}) collective-permute-start(bf16[384,512]{0,1:T(8,128)(2,1)S(1)} %collective-permute-done.12), channel_id=1, source_target_pairs={{0,2},{2,4},{4,6},{6,8},{8,10},{10,12},{12,14},{14,16},{16,18},{18... | collective-permute-start | bytes 1179656 | tf_op jit(solution)/shard_map/ppermute | solution.py:14
  48.8 7.3 collective-permute-start.6
  56.2 7.3 collective-permute-start.7
  63.5 28.6 %copy-start.6 = (bf16[384,512]{0,1:T(8,128)(2,1)}, bf16[384,512]{0,1:T(8,128)(2,1)S(1)}, u32[]{:S(2)}) copy-start(bf16[384,512]{0,1:T(8,128)(2,1)S(1)} %collective-permute-done.8) | copy-start | bytes 1179652
  63.5 15.7 %collective-permute-start.9 = (bf16[384,512]{0,1:T(8,128)(2,1)S(1)}, bf16[384,512]{0,1:T(8,128)(2,1)S(1)}, u32[]{:S(2)}, u32[]{:S(2)}) collective-permute-start(bf16[384,512]{0,1:T(8,128)(2,1)S(1)} %collective-permute-done.8), channel_id=1, source_target_pairs={{0,2},{2,4},{4,6},{6,8},{8,10},{10,12},{12,14},{14,16},{16,18},{18... | collective-permute-start | bytes 1179656 | tf_op jit(solution)/shard_map/ppermute | solution.py:14
  65.4 22.2 %copy-start.9 = (bf16[384,512]{0,1:T(8,128)(2,1)}, bf16[384,512]{0,1:T(8,128)(2,1)S(1)}, u32[]{:S(2)}) copy-start(bf16[384,512]{0,1:T(8,128)(2,1)S(1)} %collective-permute-done.13) | copy-start | bytes 1179652
  65.4 22.2 %collective-permute-start.14 = (bf16[384,512]{0,1:T(8,128)(2,1)S(1)}, bf16[384,512]{0,1:T(8,128)(2,1)S(1)}, u32[]{:S(2)}, u32[]{:S(2)}) collective-permute-start(bf16[384,512]{0,1:T(8,128)(2,1)S(1)} %collective-permute-done.13), channel_id=1, source_target_pairs={{0,2},{2,4},{4,6},{6,8},{8,10},{10,12},{12,14},{14,16},{16,18},{18... | collective-permute-start | bytes 1179656 | tf_op jit(solution)/shard_map/ppermute | solution.py:14
  79.1 27.6 %copy-start.10 = (bf16[384,512]{0,1:T(8,128)(2,1)}, bf16[384,512]{0,1:T(8,128)(2,1)S(1)}, u32[]{:S(2)}) copy-start(bf16[384,512]{0,1:T(8,128)(2,1)S(1)} %collective-permute-done.9) | copy-start | bytes 1179652
  79.1 17.0 %collective-permute-start.10 = (bf16[384,512]{0,1:T(8,128)(2,1)S(1)}, bf16[384,512]{0,1:T(8,128)(2,1)}, u32[]{:S(2)}, u32[]{:S(2)}) collective-permute-start(bf16[384,512]{0,1:T(8,128)(2,1)S(1)} %collective-permute-done.9), channel_id=1, source_target_pairs={{0,2},{2,4},{4,6},{6,8},{8,10},{10,12},{12,14},{14,16},{16,18},{18... | collective-permute-start | bytes 1179656 | tf_op jit(solution)/shard_map/ppermute | solution.py:14
  87.6 16.8 %collective-permute-start.15 = (bf16[384,512]{0,1:T(8,128)(2,1)S(1)}, bf16[384,512]{0,1:T(8,128)(2,1)S(1)}, u32[]{:S(2)}, u32[]{:S(2)}) collective-permute-start(bf16[384,512]{0,1:T(8,128)(2,1)S(1)} %collective-permute-done.14), channel_id=1, source_target_pairs={{0,2},{2,4},{4,6},{6,8},{8,10},{10,12},{12,14},{14,16},{16,18},{18... | collective-permute-start | bytes 1179656 | tf_op jit(solution)/shard_map/ppermute | solution.py:14
  92.1 20.8 %copy-start.4 = (pred[384,1920]{0,1:T(8,128)(4,1)}, pred[384,1920]{0,1:T(8,128)(4,1)S(1)}, u32[]{:S(2)}) copy-start(pred[384,1920]{0,1:T(8,128)(4,1)S(1)} %and_and_fusion) | copy-start | bytes 2211844
  92.1 38.2 %collective-permute-start.1 = (bf16[384,1024]{1,0:T(8,128)(2,1)S(1)}, bf16[384,1024]{1,0:T(8,128)(2,1)S(1)}, u32[]{:S(2)}, u32[]{:S(2)}) collective-permute-start(bf16[384,1024]{1,0:T(8,128)(2,1)S(1)} %collective-permute-done), channel_id=1, source_target_pairs={{0,2},{2,4},{4,6},{6,8},{8,10},{10,12},{12,14},{14,16},{16,18},{18... | collective-permute-start | bytes 2359304 | tf_op jit(solution)/shard_map/ppermute | solution.py:14
  96.1 36.2 %collective-permute-start.11 = (bf16[384,512]{0,1:T(8,128)(2,1)}, bf16[384,512]{0,1:T(8,128)(2,1)}, u32[]{:S(2)}, u32[]{:S(2)}) collective-permute-start(bf16[384,512]{0,1:T(8,128)(2,1)} %collective-permute-done.10), channel_id=1, source_target_pairs={{0,2},{2,4},{4,6},{6,8},{8,10},{10,12},{12,14},{14,16},{16,18},{18... | collective-permute-start | bytes 1179656 | tf_op jit(solution)/shard_map/ppermute | solution.py:14
  112.9 22.6 %copy-start.7 = (bf16[384,512]{0,1:T(8,128)(2,1)S(1)}, bf16[384,512]{0,1:T(8,128)(2,1)}, u32[]{:S(2)}) copy-start(bf16[384,512]{0,1:T(8,128)(2,1)} %copy-done.6) | copy-start | bytes 1179652
  130.3 17.8 %collective-permute-start.2 = (bf16[384,1024]{1,0:T(8,128)(2,1)S(1)}, bf16[384,1024]{1,0:T(8,128)(2,1)S(1)}, u32[]{:S(2)}, u32[]{:S(2)}) collective-permute-start(bf16[384,1024]{1,0:T(8,128)(2,1)S(1)} %collective-permute-done.1), channel_id=1, source_target_pairs={{0,2},{2,4},{4,6},{6,8},{8,10},{10,12},{12,14},{14,16},{16,18},{18... | collective-permute-start | bytes 2359304 | tf_op jit(solution)/shard_map/ppermute | solution.py:14
  148.1 19.8 %collective-permute-start.3 = (bf16[384,1024]{1,0:T(8,128)(2,1)S(1)}, bf16[384,1024]{1,0:T(8,128)(2,1)S(1)}, u32[]{:S(2)}, u32[]{:S(2)}) collective-permute-start(bf16[384,1024]{1,0:T(8,128)(2,1)S(1)} %collective-permute-done.2), channel_id=1, source_target_pairs={{0,2},{2,4},{4,6},{6,8},{8,10},{10,12},{12,14},{14,16},{16,18},{18... | collective-permute-start | bytes 2359304 | tf_op jit(solution)/shard_map/ppermute | solution.py:14
  187.0 19.7 %copy-start.14 = (bf16[384,1024]{1,0:T(8,128)(2,1)S(1)}, bf16[384,1024]{1,0:T(8,128)(2,1)}, u32[]{:S(2)}) copy-start(bf16[384,1024]{1,0:T(8,128)(2,1)} %param.14) | copy-start | bytes 2359300
  194.9 31.1 %all-gather.8.cloned.1.call-start = ((), (), s32[]{:S(2)}) async-start(), calls=%async_computation.2 | async-start | bytes 2359296 | tf_op jit(solution)/shard_map/all_gather | solution.py:88
  214.9 165.4 %all-gather.10.cloned.1.call-start = ((), (), s32[]{:S(2)}) async-start(), calls=%async_computation.3 | async-start | bytes 13369344 | tf_op jit(solution)/shard_map/all_gather | solution.py:91
  215.7 316.9 %all-gather.12.cloned.1.call-start = ((), (), s32[]{:S(2)}) async-start(), calls=%async_computation.4 | async-start | bytes 13369344 | tf_op jit(solution)/shard_map/all_gather | solution.py:96
  216.2 512.5 %all-gather.14.cloned.1.call-start = ((), (), s32[]{:S(2)}) async-start(), calls=%async_computation.5 | async-start | bytes 13369344 | tf_op jit(solution)/shard_map/all_gather | solution.py:102
  216.8 541.5 %reduce-scatter.2.cloned.1.call-start = ((), (), s32[]{:S(2)}) async-start(), calls=%async_computation.6 | async-start | bytes 2359296 | tf_op jit(solution)/shard_map/reduce_scatter | solution.py:105
  226.1 502.7 %copy-start.13 = (bf16[384,2048]{1,0:T(8,128)(2,1)S(1)}, bf16[384,2048]{1,0:T(8,128)(2,1)}, u32[]{:S(2)}) copy-start(bf16[384,2048]{1,0:T(8,128)(2,1)} %all-gather.8.cloned.1.call-done) | copy-start | bytes 4718596
  728.8 31.9 %copy-start.1 = (bf16[384,512]{1,0:T(8,128)(2,1)S(1)}, bf16[384,512]{1,0:T(8,128)(2,1)}, u32[]{:S(2)}) copy-start(bf16[384,512]{1,0:T(8,128)(2,1)} %param.17) | copy-start | bytes 1179652
  (6 other events, 50.8 us)
Sparse Core Ops, SparseCore 0:
  195.1 11.5 all-gather.5
  215.0 10.9 all-gather.7
  228.8 151.4 all-gather.9
  382.9 149.5 all-gather.11
  535.1 193.6 all-gather.13
  749.9 8.3 reduce-scatter.1
where the time goes:
time: 770 us; the launch traced here: 768 us
  waiting for transfers between devices  586 us (76%)
  matrix products  62.5 us (8%)
  other arithmetic  42.2 us (5%)
  starting transfers between devices  40.8 us (5%)
  local copies, waits for them, and re-layouts  19.9 us (3%)
  between operations  13.9 us (2%)
    all_gather x1, waiting for transfers between devices, body(): lax.all_gather(down_weight, 'sp', axis=1, tiled=True)  196 us
    all_gather x1, waiting for transfers between devices, body(): lax.all_gather(gate_weight, 'sp', axis=0, tiled=True)  154 us
    all_gather x1, waiting for transfers between devices, body(): lax.all_gather(up_weight, 'sp', axis=0, tiled=True)  142 us
    ppermute x16, waiting for transfers between devices, shifted(): return lax.ppermute(value, axis, pairs)  61.9 us
    ppermute x16, starting transfers between devices, shifted(): return lax.ppermute(value, axis, pairs)  40.4 us
    sub x2, other arithmetic, weights(): score = score - jnp.max(score, axis=-1, keepdims=True)  35.1 us
    dot_general x1, matrix products, body(): jnp.dot(hidden, lax.all_gather(down_weight, 'sp', axis=1, tiled=True), pr...  21 us
  transfers between devices with their start and end apart: 22, of which 15 were waited for; matrix products, arithmetic and copies ran while one was open for 9% of the time, Pallas kernels for 0%

commit v1 on v0

--- a/solution.py
+++ b/solution.py
@@ -6,12 +6,51 @@
 HD = 128
 VD = 256
 REACH = 4
+SHARE = 4
 
 
 def shifted(value, axis, by):
     length = lax.axis_size(axis)
     pairs = [(i, i + by) for i in range(length) if 0 <= i + by < length]
     return lax.ppermute(value, axis, pairs)
+
+
+def groups(length):
+    share = SHARE if length % SHARE == 0 else 1
+    plane = [[i * share + j for j in range(share)] for i in range(length // share)]
+    across = [[i * share + j for i in range(length // share)] for j in range(share)]
+    return plane, across
+
+
+def spread(blocks):
+    length = lax.axis_size("sp")
+    share = blocks.shape[0]
+    if share == 1:
+        return blocks
+    mine = lax.rem(lax.axis_index("sp"), share)
+    own = lax.dynamic_index_in_dim(blocks, mine, 0, keepdims=True)
+    result = lax.dynamic_update_slice_in_dim(jnp.zeros_like(blocks), own, mine, 0)
+    for by in range(1, share):
+        pairs = [(i, i - i % share + (i + by) % share) for i in range(length)]
+        sent = lax.dynamic_index_in_dim(blocks, lax.rem(mine + by, share), 0, keepdims=True)
+        came = lax.ppermute(sent, "sp", pairs)
+        result = lax.dynamic_update_slice_in_dim(result, came, lax.rem(mine + share - by, share), 0)
+    return result
+
+
+def gathered(gate_weight, up_weight, down_weight):
+    plane, across = groups(lax.axis_size("sp"))
+    share = len(plane[0])
+    depth, units = gate_weight.shape
+    part = units // share
+    both = [gate_weight.reshape(depth, share, part), up_weight.reshape(depth, share, part)]
+    both = jnp.concatenate(both, 2).transpose(1, 0, 2)
+    both = spread(both).reshape(share * depth, 2 * part)
+    down = spread(down_weight.reshape(share, part, depth))
+    down = down.transpose(1, 0, 2).reshape(part, share * depth)
+    both = lax.all_gather(both, "sp", axis=0, tiled=True, axis_index_groups=across)
+    down = lax.all_gather(down, "sp", axis=1, tiled=True, axis_index_groups=across)
+    return both, down
 
 
 def body(
@@ -33,6 +72,7 @@
     rows = query_one.shape[0]
     heads = mix_lambda.shape[0]
     position = lax.axis_index("sp")
+    both_all, down_all = gathered(gate_weight, up_weight, down_weight)
     carried = (key_one, key_two, values, segments)
     earlier = [carried]
     for step in range(REACH):
@@ -73,6 +113,7 @@
         .reshape(rows, heads * VD)
         .astype(jnp.bfloat16)
     )
+    attn_rows, both_all, down_all = lax.optimization_barrier((attn_rows, both_all, down_all))
     projected = jnp.dot(
         lax.all_gather(attn_rows, "tp", axis=1, tiled=True),
         out_weight,
@@ -85,27 +126,24 @@
     normed = (midf * lax.rsqrt(squares / channels + 1e-06)[:, None] * mixer_gain).astype(
         jnp.bfloat16
     )
+    plane, across = groups(lax.axis_size("sp"))
+    share = len(plane[0])
+    if share > 1:
+        normed = lax.all_gather(normed, "sp", axis=0, tiled=True, axis_index_groups=plane)
     whole_rows = lax.all_gather(normed, "tp", axis=1, tiled=True)
-    gate = jnp.dot(
-        whole_rows,
-        lax.all_gather(gate_weight, "sp", axis=0, tiled=True),
-        preferred_element_type=jnp.float32,
-    )
-    up = jnp.dot(
-        whole_rows,
-        lax.all_gather(up_weight, "sp", axis=0, tiled=True),
-        preferred_element_type=jnp.float32,
-    )
+    part = both_all.shape[1] // 2
+    gate = jnp.dot(whole_rows, both_all[:, :part], preferred_element_type=jnp.float32)
+    up = jnp.dot(whole_rows, both_all[:, part:], preferred_element_type=jnp.float32)
     hidden = (jax.nn.silu(gate) * up).astype(jnp.bfloat16)
-    terms = jnp.dot(
-        hidden,
-        lax.all_gather(down_weight, "sp", axis=1, tiled=True),
-        preferred_element_type=jnp.float32,
-    )
+    terms = jnp.dot(hidden, down_all, preferred_element_type=jnp.float32)
     summed = lax.psum_scatter(
         terms.astype(jnp.bfloat16), "tp", scatter_dimension=1, tiled=True
-    ).astype(jnp.float32)
-    return (midf + summed).astype(jnp.bfloat16)
+    )
+    if share > 1:
+        summed = lax.psum_scatter(
+            summed, "sp", scatter_dimension=0, tiled=True, axis_index_groups=plane
+        )
+    return (midf + summed.astype(jnp.float32)).astype(jnp.bfloat16)
 
 
 def solution(mesh):

time: 770 us -> 559 us (0.73)
  waiting for transfers between devices: 586 us -> 344 us
  local copies, waits for them, and re-layouts: 19.9 us -> 38.7 us
  starting transfers between devices: 40.8 us -> 56 us
  matrix products: 62.5 us -> 54.5 us
    all_gather x3, waiting for transfers between devices: 493 us -> 44.9 us  [the longest x1 44.9 us: body(): lax.all_gather(normed, 'sp', axis=0, tiled=True, axis_index_groups=plane)]
    ppermute x16, waiting for transfers between devices: 61.9 us -> 180 us  [shifted(): return lax.ppermute(value, axis, pairs)]
    reduce_scatter x0 -> x1, waiting for transfers between devices: none -> 47.8 us  [body(): lax.psum_scatter(summed, 'sp', scatter_dimension=0, tiled=True, axis_inde...]
    ppermute x0 -> x6, waiting for transfers between devices: none -> 28.2 us  [spread(): came = lax.ppermute(sent, 'sp', pairs)]
    all_gather x1, waiting for transfers between devices: 9.18 us -> 18.4 us  [body(): whole_rows = lax.all_gather(normed, 'tp', axis=1, tiled=True)]
    dot_general x2 -> x3, matrix products: 30.9 us -> 23 us  [the longest x1 8.21 us: body(): jnp.dot(whole_rows, both_all[:, :part], preferred_element_type=jnp.float32)]
    unnamed x50 -> x56, local copies, waits for them, and re-layouts: 11.8 us -> 18.6 us
  transfers between devices with their start and end apart: 22 -> 29, of which waited for: 15 -> 17; matrix products, arithmetic and copies ran while one was open for 9% -> 19% of each run, Pallas kernels for 0% -> 0%
where the time goes in v1:
time: 559 us; the launch traced here: 556 us
  waiting for transfers between devices  344 us (62%)
  starting transfers between devices  56 us (10%)
  matrix products  54.5 us (10%)
  other arithmetic  46.2 us (8%)
  local copies, waits for them, and re-layouts  38.7 us (7%)
  between operations  14.1 us (3%)
    ppermute x16, waiting for transfers between devices, shifted(): return lax.ppermute(value, axis, pairs)  180 us
    ppermute x16, starting transfers between devices, shifted(): return lax.ppermute(value, axis, pairs)  48 us
    reduce_scatter x1, waiting for transfers between devices, body(): lax.psum_scatter(summed, 'sp', scatter_dimension=0, tiled=True, axis_inde...  47.8 us
    all_gather x1, waiting for transfers between devices, body(): lax.all_gather(normed, 'sp', axis=0, tiled=True, axis_index_groups=plane)  44.9 us
    sub x2, other arithmetic, weights(): score = score - jnp.max(score, axis=-1, keepdims=True)  35.7 us
    ppermute x6, waiting for transfers between devices, spread(): came = lax.ppermute(sent, 'sp', pairs)  28.2 us
    unnamed x56, local copies, waits for them, and re-layouts  18.6 us
    all_gather x1, waiting for transfers between devices, body(): whole_rows = lax.all_gather(normed, 'tp', axis=1, tiled=True)  18.4 us
  transfers between devices with their start and end apart: 29, of which 17 were waited for; matrix products, arithmetic and copies ran while one was open for 19% of the time, Pallas kernels for 0%

profile of v1, /device:TPU:16, one launch (start us, length us, event | category | flops | bytes accessed | tf_op | source)
XLA Modules:
  0.0 556.0 jit_solution(11701896504892846100)
XLA Ops:
  13.3 4.3 collective-permute-done.19
  26.5 4.4 collective-permute-start.12
  34.2 4.8 collective-permute-start.8
  43.6 4.4 collective-permute-start.5
  48.0 68.8 %collective-permute-done.5 = s32[384]{0:T(512)S(1)} collective-permute-done((s32[384]{0:T(512)S(1)}, s32[384]{0:T(512)S(1)}, u32[]{:S(2)}, u32[]{:S(2)}) %collective-permute-start.5) | collective-permute-done | bytes 1568 | tf_op jit(solution)/shard_map/ppermute | solution.py:15
  119.3 4.8 collective-permute-done.6
  144.1 3.8 collective-permute-done.13
  147.8 3.6 collective-permute-start.14
  151.4 21.9 %collective-permute-done.17 = bf16[1,128,1536]{2,1,0:T(8,128)(2,1)S(1)} collective-permute-done((bf16[1,128,1536]{2,1,0:T(8,128)(2,1)S(1)}, bf16[1,128,1536]{2,1,0:T(8,128)(2,1)S(1)}, u32[]{:S(2)}, u32[]{:S(2)}) %collective-permute-start.17) | collective-permute-done | bytes 393248 | tf_op jit(solution)/shard_map/ppermute | solution.py:36
  179.5 6.5 %collective-permute-start.15 = (bf16[384,512]{0,1:T(8,128)(2,1)}, bf16[384,512]{0,1:T(8,128)(2,1)S(1)}, u32[]{:S(2)}, u32[]{:S(2)}) collective-permute-start(bf16[384,512]{0,1:T(8,128)(2,1)} %collective-permute-done.14), channel_id=1, source_target_pairs={{0,2},{2,4},{4,6},{6,8},{8,10},{10,12},{12,14},{14,16},{16,18},{18... | collective-permute-start | bytes 1179656 | tf_op jit(solution)/shard_map/ppermute | solution.py:15
  186.0 3.7 and_and_fusion
  189.8 14.5 %collective-permute-done.10 = bf16[384,512]{0,1:T(8,128)(2,1)S(1)} collective-permute-done((bf16[384,512]{0,1:T(8,128)(2,1)}, bf16[384,512]{0,1:T(8,128)(2,1)S(1)}, u32[]{:S(2)}, u32[]{:S(2)}) %collective-permute-start.10) | collective-permute-done | bytes 393248 | tf_op jit(solution)/shard_map/ppermute | solution.py:15
  206.2 19.1 %collective-permute-done.15 = bf16[384,512]{0,1:T(8,128)(2,1)S(1)} collective-permute-done((bf16[384,512]{0,1:T(8,128)(2,1)}, bf16[384,512]{0,1:T(8,128)(2,1)S(1)}, u32[]{:S(2)}, u32[]{:S(2)}) %collective-permute-start.15) | collective-permute-done | bytes 393248 | tf_op jit(solution)/shard_map/ppermute | solution.py:15
  230.8 16.8 %collective-permute-done.11 = bf16[384,512]{0,1:T(8,128)(2,1)S(1)} collective-permute-done((bf16[384,512]{0,1:T(8,128)(2,1)S(1)}, bf16[384,512]{0,1:T(8,128)(2,1)S(1)}, u32[]{:S(2)}, u32[]{:S(2)}) %collective-permute-start.11) | collective-permute-done | bytes 393248 | tf_op jit(solution)/shard_map/ppermute | solution.py:15
  248.7 6.1 %fusion.26 = f32[4,1920,384]{2,1,0:T(8,128)} fusion(bf16[1920,4,128]{0,2,1:T(8,128)(2,1)S(1)} %bitcast.78, bf16[384,512]{1,0:T(8,128)(2,1)S(1)} %copy-done), kind=kOutput, calls=%fused_computation.50 | convolution fusion | flops 754974720 | bytes 14155776 | tf_op jit(solution)/shard_map/qhd,khd->hqk/dot_general | solution.py:95
  254.9 17.9 %fusion.36 = (f32[4,384]{1,0:T(4,128)S(1)}, f32[4,384,1920]{1,2,0:T(8,128)}) fusion(f32[4,1920,384]{2,1,0:T(8,128)} %fusion.26, pred[384,1920]{0,1:T(8,128)(4,1)} %and_and_fusion), kind=kOutput, calls=%fused_computation.97 | output fusion | flops 17696640 | bytes 24336384 | tf_op jit(solution)/shard_map/sub | solution.py:99
  273.9 6.1 %fusion.29 = f32[4,1920,384]{2,1,0:T(8,128)} fusion(bf16[1920,4,128]{0,2,1:T(8,128)(2,1)S(1)} %bitcast.79, bf16[384,512]{1,0:T(8,128)(2,1)S(1)} %copy-done.7), kind=kOutput, calls=%fused_computation.53 | convolution fusion | flops 754974720 | bytes 14155776 | tf_op jit(solution)/shard_map/qhd,khd->hqk/dot_general | solution.py:95
  280.0 15.1 %collective-permute-done.2 = bf16[384,1024]{1,0:T(8,128)(2,1)} collective-permute-done((bf16[384,1024]{1,0:T(8,128)(2,1)S(1)}, bf16[384,1024]{1,0:T(8,128)(2,1)}, u32[]{:S(2)}, u32[]{:S(2)}) %collective-permute-start.2) | collective-permute-done | bytes 786464 | tf_op jit(solution)/shard_map/ppermute | solution.py:15
  297.2 17.8 %fusion.37 = (f32[4,384]{1,0:T(4,128)S(1)}, f32[4,384,1920]{1,2,0:T(8,128)}) fusion(f32[4,1920,384]{2,1,0:T(8,128)} %fusion.29, pred[384,1920]{0,1:T(8,128)(4,1)} %and_and_fusion), kind=kOutput, calls=%fused_computation.98 | output fusion | flops 17696640 | bytes 24336384 | tf_op jit(solution)/shard_map/sub | solution.py:99
  315.1 34.4 %collective-permute-done.3 = bf16[384,1024]{1,0:T(8,128)(2,1)S(1)} collective-permute-done((bf16[384,1024]{1,0:T(8,128)(2,1)}, bf16[384,1024]{1,0:T(8,128)(2,1)S(1)}, u32[]{:S(2)}, u32[]{:S(2)}) %collective-permute-start.3) | collective-permute-done | bytes 786464 | tf_op jit(solution)/shard_map/ppermute | solution.py:15
  357.6 6.2 %copy.31 = bf16[1920,1024]{0,1:T(8,128)(2,1)} copy(bf16[1920,1024]{1,0:T(8,128)(2,1)} %constant_dynamic-update-slice_fusion) | data formatting | bytes 7864320 | tf_op jit(solution)/shard_map/concatenate | solution.py:84
  363.9 8.0 %fusion.9 = f32[4,256,384]{2,1,0:T(8,128)S(1)} fusion(bf16[1920,4,256]{0,2,1:T(8,128)(2,1)} %bitcast.72, f32[4,384,1920]{1,2,0:T(8,128)} %get-tuple-element.20, f32[4,384]{1,0:T(4,128)S(1)} %get-tuple-element.19), kind=kOutput, calls=%fused_computation.16 | convolution fusion | flops 1515847680 | bytes 17307648 | tf_op jit(solution)/shard_map/hqk,khe->qhe/dot_general | solution.py:106
  371.9 6.7 %fusion.19 = (f32[384,4]{0,1:T(4,128)S(1)}, f32[4,256,384]{2,1,0:T(8,128)S(1)}) fusion(f32[4,256,384]{2,1,0:T(8,128)S(1)} %fusion.9, f32[4]{0:T(128)S(1)} %copy-done.17, bf16[1920,4,256]{0,2,1:T(8,128)(2,1)S(1)} %bitcast.73, f32[4,384,1920]{1,2,0:T(8,128)} %get-tuple-element.22, f32[4,384]{1,0:T(4,128)S(1)} %get-tuple-element.21), kind=kOutput, calls=%fused_computation.41 | convolution fusion | flops 1517419008 | bytes 18886672 | tf_op jit(solution)/shard_map/hqk,khe->qhe/dot_general | solution.py:103
  380.0 9.0 %all-gather.10.cloned.1.call-done = bf16[384,2048]{0,1:T(8,128)(2,1)} async-done(((bf16[384,1024]{0,1:T(8,128)(2,1)}), bf16[384,2048]{0,1:T(8,128)(2,1)}) %all-gather.10.cloned.1.call-update) | async-done | bytes 1572880 | tf_op jit(solution)/shard_map/all_gather | solution.py:118
  389.0 4.6 fusion.15
  397.3 44.9 %all-gather.12.cloned.1.call-done = bf16[1536,1024]{1,0:T(8,128)(2,1)} async-done(((bf16[384,1024]{1,0:T(8,128)(2,1)}), bf16[1536,1024]{1,0:T(8,128)(2,1)}) %all-gather.12.cloned.1.call-update) | async-done | bytes 3145744 | tf_op jit(solution)/shard_map/all_gather | solution.py:132
  442.3 18.4 %all-gather.14.cloned.1.call-done = bf16[1536,2048]{1,0:T(8,128)(2,1)} async-done(((bf16[1536,1024]{1,0:T(8,128)(2,1)}), bf16[1536,2048]{1,0:T(8,128)(2,1)}) %all-gather.14.cloned.1.call-update) | async-done | bytes 6291472 | tf_op jit(solution)/shard_map/all_gather | solution.py:133
  460.6 8.2 %fusion.13 = f32[1536,768]{1,0:T(8,128)S(1)} fusion(bf16[1536,2048]{1,0:T(8,128)(2,1)} %all-gather.14.cloned.1.call-done, bf16[2048,1536]{1,0:T(8,128)(2,1)} %all-gather.6.cloned.1.call-done), kind=kOutput, calls=%fused_computation.21 | convolution fusion | flops 4831838208 | bytes 14155776 | tf_op jit(solution)/shard_map/dot_general | solution.py:135
  468.9 7.7 %multiply_convert_fusion = bf16[1536,768]{1,0:T(8,128)(2,1)S(1)} fusion(f32[1536,768]{1,0:T(8,128)S(1)} %fusion.13, bf16[1536,2048]{1,0:T(8,128)(2,1)S(1)} %copy-done.14, bf16[2048,1536]{1,0:T(8,128)(2,1)} %all-gather.6.cloned.1.call-done), kind=kOutput, calls=%fused_computation.19 | convolution fusion | flops 4838916096 | bytes 16515072 | tf_op jit(solution)/shard_map/dot_general | solution.py:136
  476.6 7.1 %convolution_convert_fusion = bf16[1536,2048]{1,0:T(8,128)(2,1)} fusion(bf16[1536,768]{1,0:T(8,128)(2,1)S(1)} %multiply_convert_fusion, bf16[768,2048]{0,1:T(8,128)(2,1)S(1)} %copy-done.15), kind=kOutput, calls=%fused_computation.10 | convolution fusion | flops 4834983936 | bytes 11796480 | tf_op jit(solution)/shard_map/dot_general | solution.py:138
  483.8 15.2 %reduce-scatter.3.cloned.1.call-done = bf16[1536,1024]{1,0:T(8,128)(2,1)} async-done(((bf16[1536,2048]{1,0:T(8,128)(2,1)}), bf16[1536,1024]{1,0:T(8,128)(2,1)}) %reduce-scatter.3.cloned.1.call-update) | async-done | bytes 3145744 | tf_op jit(solution)/shard_map/reduce_scatter | solution.py:139
  499.0 47.8 %reduce-scatter.5.cloned.1.call-done = bf16[384,1024]{1,0:T(8,128)(2,1)} async-done(((bf16[1536,1024]{1,0:T(8,128)(2,1)}), bf16[384,1024]{1,0:T(8,128)(2,1)}) %reduce-scatter.5.cloned.1.call-update) | async-done | bytes 786448 | tf_op jit(solution)/shard_map/reduce_scatter | solution.py:143
  (135 shorter events, 79.1 us)
Async XLA Ops:
  6.5 242.2 %copy-start = (bf16[384,512]{1,0:T(8,128)(2,1)S(1)}, bf16[384,512]{1,0:T(8,128)(2,1)}, u32[]{:S(2)}) copy-start(bf16[384,512]{1,0:T(8,128)(2,1)} %param.17) | copy-start | bytes 1179652
  6.5 373.1 %all-gather.8.cloned.1.call-start = ((), (), s32[]{:S(2)}) async-start(), calls=%async_computation.3 | async-start | bytes 3932160 | tf_op jit(solution)/shard_map/all_gather | solution.py:52
  8.6 9.0 %collective-permute-start.19 = (bf16[1,768,128]{2,1,0:T(8,128)(2,1)}, bf16[1,768,128]{2,1,0:T(8,128)(2,1)}, u32[]{:S(2)}, u32[]{:S(2)}) collective-permute-start(bf16[1,768,128]{2,1,0:T(8,128)(2,1)} %get-tuple-element.17), channel_id=1, source_target_pairs={{0,2},{2,4},{4,6},{6,0},{8,10},{10,12},{12,14},{14,8},{16,18},{18,... | collective-permute-start | bytes 589832 | tf_op jit(solution)/shard_map/ppermute | solution.py:36
  10.1 10.6 %collective-permute-start.20 = (bf16[1,768,128]{2,1,0:T(8,128)(2,1)S(1)}, bf16[1,768,128]{2,1,0:T(8,128)(2,1)}, u32[]{:S(2)}, u32[]{:S(2)}) collective-permute-start(bf16[1,768,128]{2,1,0:T(8,128)(2,1)S(1)} %get-tuple-element.16), channel_id=1, source_target_pairs={{0,4},{2,6},{4,0},{6,2},{8,12},{10,14},{12,8},{14,10},{16,20},{18,... | collective-permute-start | bytes 589832 | tf_op jit(solution)/shard_map/ppermute | solution.py:36
  11.6 10.2 %collective-permute-start.21 = (bf16[1,768,128]{2,1,0:T(8,128)(2,1)}, bf16[1,768,128]{2,1,0:T(8,128)(2,1)}, u32[]{:S(2)}, u32[]{:S(2)}) collective-permute-start(bf16[1,768,128]{2,1,0:T(8,128)(2,1)} %get-tuple-element.15), channel_id=1, source_target_pairs={{0,6},{2,0},{4,2},{6,4},{8,14},{10,8},{12,10},{14,12},{16,22},{18,... | collective-permute-start | bytes 589832 | tf_op jit(solution)/shard_map/ppermute | solution.py:36
  23.9 355.8 %all-gather.6.cloned.1.call-start = ((), (), s32[]{:S(2)}) async-start(), calls=%async_computation.2 | async-start | bytes 7864320 | tf_op jit(solution)/shard_map/all_gather | solution.py:51
  23.9 19.6 %collective-permute-start.4 = (s32[384]{0:T(512)S(1)}, s32[384]{0:T(512)S(1)}, u32[]{:S(2)}, u32[]{:S(2)}) collective-permute-start(s32[384]{0:T(512)S(1)} %copy-done.9), channel_id=1, source_target_pairs={{0,2},{2,4},{4,6},{6,8},{8,10},{10,12},{12,14},{14,16},{16,18},{18... | collective-permute-start | bytes 4616 | tf_op jit(solution)/shard_map/ppermute | solution.py:15
  26.5 107.3 %collective-permute-start.12 = (bf16[384,512]{0,1:T(8,128)(2,1)S(1)}, bf16[384,512]{0,1:T(8,128)(2,1)}, u32[]{:S(2)}, u32[]{:S(2)}) collective-permute-start(bf16[384,512]{0,1:T(8,128)(2,1)S(1)} %copy.37), channel_id=1, source_target_pairs={{0,2},{2,4},{4,6},{6,8},{8,10},{10,12},{12,14},{14,16},{16,18},{18... | collective-permute-start | bytes 1179656 | tf_op jit(solution)/shard_map/ppermute | solution.py:15
  31.0 142.4 %collective-permute-start = (bf16[384,1024]{1,0:T(8,128)(2,1)}, bf16[384,1024]{1,0:T(8,128)(2,1)}, u32[]{:S(2)}, u32[]{:S(2)}) collective-permute-start(bf16[384,1024]{1,0:T(8,128)(2,1)} %param.19), channel_id=1, source_target_pairs={{0,2},{2,4},{4,6},{6,8},{8,10},{10,12},{12,14},{14,16},{16,18},{18... | collective-permute-start | bytes 2359304 | tf_op jit(solution)/shard_map/ppermute | solution.py:15
  34.2 104.4 %collective-permute-start.8 = (bf16[384,512]{0,1:T(8,128)(2,1)S(1)}, bf16[384,512]{0,1:T(8,128)(2,1)}, u32[]{:S(2)}, u32[]{:S(2)}) collective-permute-start(bf16[384,512]{0,1:T(8,128)(2,1)S(1)} %copy.32), channel_id=1, source_target_pairs={{0,2},{2,4},{4,6},{6,8},{8,10},{10,12},{12,14},{14,16},{16,18},{18... | collective-permute-start | bytes 1179656 | tf_op jit(solution)/shard_map/ppermute | solution.py:15
  41.7 99.4 %collective-permute-start.16 = (bf16[1,128,1536]{2,1,0:T(8,128)(2,1)}, bf16[1,128,1536]{2,1,0:T(8,128)(2,1)}, u32[]{:S(2)}, u32[]{:S(2)}) collective-permute-start(bf16[1,128,1536]{2,1,0:T(8,128)(2,1)} %bitcast.10), channel_id=1, source_target_pairs={{0,2},{2,4},{4,6},{6,0},{8,10},{10,12},{12,14},{14,8},{16,18},{18,... | collective-permute-start | bytes 1179656 | tf_op jit(solution)/shard_map/ppermute | solution.py:36
  43.5 82.5 %copy-start.11 = (s32[384]{0:T(512)}, s32[384]{0:T(512)S(1)}, u32[]{:S(2)}) copy-start(s32[384]{0:T(512)S(1)} %collective-permute-done.4) | copy-start | bytes 4612
  43.6 73.2 %collective-permute-start.5 = (s32[384]{0:T(512)S(1)}, s32[384]{0:T(512)S(1)}, u32[]{:S(2)}, u32[]{:S(2)}) collective-permute-start(s32[384]{0:T(512)S(1)} %collective-permute-done.4), channel_id=1, source_target_pairs={{0,2},{2,4},{4,6},{6,8},{8,10},{10,12},{12,14},{14,16},{16,18},{18... | collective-permute-start | bytes 4616 | tf_op jit(solution)/shard_map/ppermute | solution.py:15
  116.8 7.4 %collective-permute-start.6 = (s32[384]{0:T(512)S(1)}, s32[384]{0:T(512)}, u32[]{:S(2)}, u32[]{:S(2)}) collective-permute-start(s32[384]{0:T(512)S(1)} %collective-permute-done.5), channel_id=1, source_target_pairs={{0,2},{2,4},{4,6},{6,8},{8,10},{10,12},{12,14},{14,16},{16,18},{18... | collective-permute-start | bytes 4616 | tf_op jit(solution)/shard_map/ppermute | solution.py:15
  124.2 7.7 %collective-permute-start.7 = (s32[384]{0:T(512)}, s32[384]{0:T(512)}, u32[]{:S(2)}, u32[]{:S(2)}) collective-permute-start(s32[384]{0:T(512)} %collective-permute-done.6), channel_id=1, source_target_pairs={{0,2},{2,4},{4,6},{6,8},{8,10},{10,12},{12,14},{14,16},{16,18},{18... | collective-permute-start | bytes 4616 | tf_op jit(solution)/shard_map/ppermute | solution.py:15
  131.8 41.5 %collective-permute-start.17 = (bf16[1,128,1536]{2,1,0:T(8,128)(2,1)S(1)}, bf16[1,128,1536]{2,1,0:T(8,128)(2,1)S(1)}, u32[]{:S(2)}, u32[]{:S(2)}) collective-permute-start(bf16[1,128,1536]{2,1,0:T(8,128)(2,1)S(1)} %bitcast.81), channel_id=1, source_target_pairs={{0,4},{2,6},{4,0},{6,2},{8,12},{10,14},{12,8},{14,10},{16,20},{18,... | collective-permute-start | bytes 1179656 | tf_op jit(solution)/shard_map/ppermute | solution.py:36
  133.9 14.0 %collective-permute-start.13 = (bf16[384,512]{0,1:T(8,128)(2,1)}, bf16[384,512]{0,1:T(8,128)(2,1)}, u32[]{:S(2)}, u32[]{:S(2)}) collective-permute-start(bf16[384,512]{0,1:T(8,128)(2,1)} %collective-permute-done.12), channel_id=1, source_target_pairs={{0,2},{2,4},{4,6},{6,8},{8,10},{10,12},{12,14},{14,16},{16,18},{18... | collective-permute-start | bytes 1179656 | tf_op jit(solution)/shard_map/ppermute | solution.py:15
  138.6 36.7 %collective-permute-start.18 = (bf16[1,128,1536]{2,1,0:T(8,128)(2,1)}, bf16[1,128,1536]{2,1,0:T(8,128)(2,1)S(1)}, u32[]{:S(2)}, u32[]{:S(2)}) collective-permute-start(bf16[1,128,1536]{2,1,0:T(8,128)(2,1)} %bitcast.12), channel_id=1, source_target_pairs={{0,6},{2,0},{4,2},{6,4},{8,14},{10,8},{12,10},{14,12},{16,22},{18,... | collective-permute-start | bytes 1179656 | tf_op jit(solution)/shard_map/ppermute | solution.py:36
  141.1 35.5 %collective-permute-start.9 = (bf16[384,512]{0,1:T(8,128)(2,1)}, bf16[384,512]{0,1:T(8,128)(2,1)}, u32[]{:S(2)}, u32[]{:S(2)}) collective-permute-start(bf16[384,512]{0,1:T(8,128)(2,1)} %collective-permute-done.8), channel_id=1, source_target_pairs={{0,2},{2,4},{4,6},{6,8},{8,10},{10,12},{12,14},{14,16},{16,18},{18... | collective-permute-start | bytes 1179656 | tf_op jit(solution)/shard_map/ppermute | solution.py:15
  147.8 31.7 %collective-permute-start.14 = (bf16[384,512]{0,1:T(8,128)(2,1)}, bf16[384,512]{0,1:T(8,128)(2,1)}, u32[]{:S(2)}, u32[]{:S(2)}) collective-permute-start(bf16[384,512]{0,1:T(8,128)(2,1)} %collective-permute-done.13), channel_id=1, source_target_pairs={{0,2},{2,4},{4,6},{6,8},{8,10},{10,12},{12,14},{14,16},{16,18},{18... | collective-permute-start | bytes 1179656 | tf_op jit(solution)/shard_map/ppermute | solution.py:15
  173.4 53.1 %collective-permute-start.1 = (bf16[384,1024]{1,0:T(8,128)(2,1)}, bf16[384,1024]{1,0:T(8,128)(2,1)S(1)}, u32[]{:S(2)}, u32[]{:S(2)}) collective-permute-start(bf16[384,1024]{1,0:T(8,128)(2,1)} %collective-permute-done), channel_id=1, source_target_pairs={{0,2},{2,4},{4,6},{6,8},{8,10},{10,12},{12,14},{14,16},{16,18},{18... | collective-permute-start | bytes 2359304 | tf_op jit(solution)/shard_map/ppermute | solution.py:15
  176.5 212.5 %all-gather.10.cloned.1.call-start = ((), (), s32[]{:S(2)}) async-start(), calls=%async_computation.4 | async-start | bytes 2359296 | tf_op jit(solution)/shard_map/all_gather | solution.py:118
  176.6 27.7 %collective-permute-start.10 = (bf16[384,512]{0,1:T(8,128)(2,1)}, bf16[384,512]{0,1:T(8,128)(2,1)S(1)}, u32[]{:S(2)}, u32[]{:S(2)}) collective-permute-start(bf16[384,512]{0,1:T(8,128)(2,1)} %collective-permute-done.9), channel_id=1, source_target_pairs={{0,2},{2,4},{4,6},{6,8},{8,10},{10,12},{12,14},{14,16},{16,18},{18... | collective-permute-start | bytes 1179656 | tf_op jit(solution)/shard_map/ppermute | solution.py:15
  179.5 45.8 %collective-permute-start.15 = (bf16[384,512]{0,1:T(8,128)(2,1)}, bf16[384,512]{0,1:T(8,128)(2,1)S(1)}, u32[]{:S(2)}, u32[]{:S(2)}) collective-permute-start(bf16[384,512]{0,1:T(8,128)(2,1)} %collective-permute-done.14), channel_id=1, source_target_pairs={{0,2},{2,4},{4,6},{6,8},{8,10},{10,12},{12,14},{14,16},{16,18},{18... | collective-permute-start | bytes 1179656 | tf_op jit(solution)/shard_map/ppermute | solution.py:15
  204.3 43.3 %collective-permute-start.11 = (bf16[384,512]{0,1:T(8,128)(2,1)S(1)}, bf16[384,512]{0,1:T(8,128)(2,1)S(1)}, u32[]{:S(2)}, u32[]{:S(2)}) collective-permute-start(bf16[384,512]{0,1:T(8,128)(2,1)S(1)} %collective-permute-done.10), channel_id=1, source_target_pairs={{0,2},{2,4},{4,6},{6,8},{8,10},{10,12},{12,14},{14,16},{16,18},{18... | collective-permute-start | bytes 1179656 | tf_op jit(solution)/shard_map/ppermute | solution.py:15
  226.5 68.6 %collective-permute-start.2 = (bf16[384,1024]{1,0:T(8,128)(2,1)S(1)}, bf16[384,1024]{1,0:T(8,128)(2,1)}, u32[]{:S(2)}, u32[]{:S(2)}) collective-permute-start(bf16[384,1024]{1,0:T(8,128)(2,1)S(1)} %collective-permute-done.1), channel_id=1, source_target_pairs={{0,2},{2,4},{4,6},{6,8},{8,10},{10,12},{12,14},{14,16},{16,18},{18... | collective-permute-start | bytes 2359304 | tf_op jit(solution)/shard_map/ppermute | solution.py:15
  295.1 54.4 %collective-permute-start.3 = (bf16[384,1024]{1,0:T(8,128)(2,1)}, bf16[384,1024]{1,0:T(8,128)(2,1)S(1)}, u32[]{:S(2)}, u32[]{:S(2)}) collective-permute-start(bf16[384,1024]{1,0:T(8,128)(2,1)} %collective-permute-done.2), channel_id=1, source_target_pairs={{0,2},{2,4},{4,6},{6,8},{8,10},{10,12},{12,14},{14,16},{16,18},{18... | collective-permute-start | bytes 2359304 | tf_op jit(solution)/shard_map/ppermute | solution.py:15
  379.7 62.5 %all-gather.12.cloned.1.call-start = ((), (), s32[]{:S(2)}) async-start(), calls=%async_computation.5 | async-start | bytes 3932160 | tf_op jit(solution)/shard_map/all_gather | solution.py:132
  397.3 63.4 %all-gather.14.cloned.1.call-start = ((), (), s32[]{:S(2)}) async-start(), calls=%async_computation.6 | async-start | bytes 9437184 | tf_op jit(solution)/shard_map/all_gather | solution.py:133
  442.2 56.8 %reduce-scatter.3.cloned.1.call-start = ((), (), s32[]{:S(2)}) async-start(), calls=%async_computation.7 | async-start | bytes 9437184 | tf_op jit(solution)/shard_map/reduce_scatter | solution.py:139
  483.7 65.4 %copy-start.1 = (bf16[384,512]{1,0:T(8,128)(2,1)S(1)}, bf16[384,512]{1,0:T(8,128)(2,1)}, u32[]{:S(2)}) copy-start(bf16[384,512]{1,0:T(8,128)(2,1)} %param.17) | copy-start | bytes 1179652
  483.7 63.1 %reduce-scatter.5.cloned.1.call-start = ((), (), s32[]{:S(2)}) async-start(), calls=%async_computation.8 | async-start | bytes 3932160 | tf_op jit(solution)/shard_map/reduce_scatter | solution.py:143
  (15 other events, 185.6 us)
Sparse Core Ops, SparseCore 0:
  24.0 62.2 all-gather.7
  176.7 120.8 all-gather.5
  379.8 9.1 all-gather.9
  397.4 44.7 all-gather.11
  443.6 17.0 all-gather.13
  483.8 15.0 reduce-scatter.2
  502.0 44.8 reduce-scatter.4

commit v2 on v1

--- a/solution.py
+++ b/solution.py
@@ -6,7 +6,7 @@
 HD = 128
 VD = 256
 REACH = 4
-SHARE = 4
+SHARE = 2
 
 
 def shifted(value, axis, by):

time: 559 us -> 560 us (level)
  waiting for transfers between devices: 344 us -> 356 us
  starting transfers between devices: 56 us -> 44.9 us
  local copies, waits for them, and re-layouts: 38.7 us -> 28.9 us
    ppermute x16, waiting for transfers between devices: 180 us -> 229 us  [shifted(): return lax.ppermute(value, axis, pairs)]
    reduce_scatter x1, waiting for transfers between devices: 47.8 us -> 29.3 us  [body(): lax.psum_scatter(summed, 'sp', scatter_dimension=0, tiled=True, axis_inde...]
    all_gather x1, waiting for transfers between devices: 44.9 us -> 28.2 us  [body(): lax.all_gather(normed, 'sp', axis=0, tiled=True, axis_index_groups=plane)]
    dot_general x1, matrix products: 7.14 us -> 18.8 us  [body(): terms = jnp.dot(hidden, down_all, preferred_element_type=jnp.float32)]
    all_gather x1, waiting for transfers between devices: 0.01 us -> 8.09 us  [gathered(): lax.all_gather(both, 'sp', axis=0, tiled=True, axis_index_groups=across)]
    dot_general x1 -> x0, matrix products: 7.66 us -> none  [body(): jnp.dot(whole_rows, both_all[:, part:], preferred_element_type=jnp.float32)]
    ppermute x16, starting transfers between devices: 48 us -> 41.5 us  [shifted(): return lax.ppermute(value, axis, pairs)]
    unnamed x56 -> x60, local copies, waits for them, and re-layouts: 18.6 us -> 15.4 us
  transfers between devices with their start and end apart: 29 -> 25, of which waited for: 17 -> 18; matrix products, arithmetic and copies ran while one was open for 19% -> 17% of each run, Pallas kernels for 0% -> 0%
where the time goes in v2:
time: 560 us; the launch traced here: 553 us
  waiting for transfers between devices  356 us (64%)
  matrix products  59.9 us (11%)
  other arithmetic  46.3 us (8%)
  starting transfers between devices  44.9 us (8%)
  local copies, waits for them, and re-layouts  28.9 us (5%)
  between operations  14.5 us (3%)
    ppermute x16, waiting for transfers between devices, shifted(): return lax.ppermute(value, axis, pairs)  229 us
    ppermute x16, starting transfers between devices, shifted(): return lax.ppermute(value, axis, pairs)  41.5 us
    sub x2, other arithmetic, weights(): score = score - jnp.max(score, axis=-1, keepdims=True)  36.8 us
    reduce_scatter x1, waiting for transfers between devices, body(): lax.psum_scatter(summed, 'sp', scatter_dimension=0, tiled=True, axis_inde...  29.3 us
    all_gather x1, waiting for transfers between devices, body(): lax.all_gather(normed, 'sp', axis=0, tiled=True, axis_index_groups=plane)  28.2 us
    ppermute x2, waiting for transfers between devices, spread(): came = lax.ppermute(sent, 'sp', pairs)  26 us
    dot_general x1, matrix products, body(): terms = jnp.dot(hidden, down_all, preferred_element_type=jnp.float32)  18.8 us
    unnamed x60, local copies, waits for them, and re-layouts  15.4 us
  transfers between devices with their start and end apart: 25, of which 18 were waited for; matrix products, arithmetic and copies ran while one was open for 17% of the time, Pallas kernels for 0%

profile of v2, /device:TPU:16, one launch (start us, length us, event | category | flops | bytes accessed | tf_op | source)
XLA Modules:
  0.0 552.9 jit_solution(14133825579626609657)
XLA Ops:
  10.3 9.3 %collective-permute-done.17 = bf16[1,1536,128]{2,1,0:T(8,128)(2,1)S(1)} collective-permute-done((bf16[1,1536,128]{2,1,0:T(8,128)(2,1)}, bf16[1,1536,128]{2,1,0:T(8,128)(2,1)S(1)}, u32[]{:S(2)}, u32[]{:S(2)}) %collective-permute-start.17) | collective-permute-done | bytes 393248 | tf_op jit(solution)/shard_map/ppermute | solution.py:36
  24.9 16.7 %collective-permute-done.16 = bf16[1,128,3072]{2,1,0:T(8,128)(2,1)} collective-permute-done((bf16[1,128,3072]{2,1,0:T(8,128)(2,1)}, bf16[1,128,3072]{2,1,0:T(8,128)(2,1)}, u32[]{:S(2)}, u32[]{:S(2)}) %collective-permute-start.16) | collective-permute-done | bytes 786464 | tf_op jit(solution)/shard_map/ppermute | solution.py:36
  45.3 3.4 collective-permute-start.12
  55.7 3.4 collective-permute-start.8
  59.2 9.3 %collective-permute-done.4 = s32[384]{0:T(512)S(1)} collective-permute-done((s32[384]{0:T(512)S(1)}, s32[384]{0:T(512)S(1)}, u32[]{:S(2)}, u32[]{:S(2)}) %collective-permute-start.4) | collective-permute-done | bytes 1568 | tf_op jit(solution)/shard_map/ppermute | solution.py:15
  72.4 53.4 %collective-permute-done.5 = s32[384]{0:T(512)S(1)} collective-permute-done((s32[384]{0:T(512)S(1)}, s32[384]{0:T(512)S(1)}, u32[]{:S(2)}, u32[]{:S(2)}) %collective-permute-start.5) | collective-permute-done | bytes 1568 | tf_op jit(solution)/shard_map/ppermute | solution.py:15
  128.3 22.0 %collective-permute-done.6 = s32[384]{0:T(512)} collective-permute-done((s32[384]{0:T(512)S(1)}, s32[384]{0:T(512)}, u32[]{:S(2)}, u32[]{:S(2)}) %collective-permute-start.6) | collective-permute-done | bytes 1568 | tf_op jit(solution)/shard_map/ppermute | solution.py:15
  152.8 5.1 collective-permute-done.7
  164.3 5.7 %collective-permute-start.1 = (bf16[384,1024]{1,0:T(8,128)(2,1)S(1)}, bf16[384,1024]{1,0:T(8,128)(2,1)}, u32[]{:S(2)}, u32[]{:S(2)}) collective-permute-start(bf16[384,1024]{1,0:T(8,128)(2,1)S(1)} %collective-permute-done), channel_id=1, source_target_pairs={{0,2},{2,4},{4,6},{6,8},{8,10},{10,12},{12,14},{14,16},{16,18},{18... | collective-permute-start | bytes 2359304 | tf_op jit(solution)/shard_map/ppermute | solution.py:15
  170.7 3.4 collective-permute-done.9
  176.8 18.3 %collective-permute-done.14 = bf16[384,512]{0,1:T(8,128)(2,1)S(1)} collective-permute-done((bf16[384,512]{0,1:T(8,128)(2,1)}, bf16[384,512]{0,1:T(8,128)(2,1)S(1)}, u32[]{:S(2)}, u32[]{:S(2)}) %collective-permute-start.14) | collective-permute-done | bytes 393248 | tf_op jit(solution)/shard_map/ppermute | solution.py:15
  197.1 3.7 and_and_fusion
  200.8 52.2 %collective-permute-done.10 = bf16[384,512]{0,1:T(8,128)(2,1)S(1)} collective-permute-done((bf16[384,512]{0,1:T(8,128)(2,1)S(1)}, bf16[384,512]{0,1:T(8,128)(2,1)S(1)}, u32[]{:S(2)}, u32[]{:S(2)}) %collective-permute-start.10) | collective-permute-done | bytes 393248 | tf_op jit(solution)/shard_map/ppermute | solution.py:15
  254.9 9.8 %collective-permute-done.15 = bf16[384,512]{0,1:T(8,128)(2,1)S(1)} collective-permute-done((bf16[384,512]{0,1:T(8,128)(2,1)S(1)}, bf16[384,512]{0,1:T(8,128)(2,1)S(1)}, u32[]{:S(2)}, u32[]{:S(2)}) %collective-permute-start.15) | collective-permute-done | bytes 393248 | tf_op jit(solution)/shard_map/ppermute | solution.py:15
  268.2 7.1 %collective-permute-done.11 = bf16[384,512]{0,1:T(8,128)(2,1)S(1)} collective-permute-done((bf16[384,512]{0,1:T(8,128)(2,1)S(1)}, bf16[384,512]{0,1:T(8,128)(2,1)S(1)}, u32[]{:S(2)}, u32[]{:S(2)}) %collective-permute-start.11) | collective-permute-done | bytes 393248 | tf_op jit(solution)/shard_map/ppermute | solution.py:15
  275.5 6.2 %fusion.29 = f32[4,1920,384]{2,1,0:T(8,128)} fusion(bf16[1920,4,128]{0,2,1:T(8,128)(2,1)S(1)} %bitcast.75, bf16[384,512]{1,0:T(8,128)(2,1)S(1)} %copy-done), kind=kOutput, calls=%fused_computation.46 | convolution fusion | flops 754974720 | bytes 14155776 | tf_op jit(solution)/shard_map/qhd,khd->hqk/dot_general | solution.py:95
  281.6 19.0 %fusion.40 = (f32[4,384]{1,0:T(4,128)S(1)}, f32[4,384,1920]{1,2,0:T(8,128)}) fusion(f32[4,1920,384]{2,1,0:T(8,128)} %fusion.29, pred[384,1920]{0,1:T(8,128)(4,1)} %and_and_fusion), kind=kOutput, calls=%fused_computation.87 | output fusion | flops 17696640 | bytes 24336384 | tf_op jit(solution)/shard_map/sub | solution.py:99
  301.8 6.2 %fusion.32 = f32[4,1920,384]{2,1,0:T(8,128)} fusion(bf16[1920,4,128]{0,2,1:T(8,128)(2,1)S(1)} %bitcast.76, bf16[384,512]{1,0:T(8,128)(2,1)S(1)} %copy-done.10), kind=kOutput, calls=%fused_computation.49 | convolution fusion | flops 754974720 | bytes 14155776 | tf_op jit(solution)/shard_map/qhd,khd->hqk/dot_general | solution.py:95
  310.1 17.8 %fusion.41 = (f32[4,384]{1,0:T(4,128)S(1)}, f32[4,384,1920]{1,2,0:T(8,128)}) fusion(f32[4,1920,384]{2,1,0:T(8,128)} %fusion.32, pred[384,1920]{0,1:T(8,128)(4,1)} %and_and_fusion), kind=kOutput, calls=%fused_computation.88 | output fusion | flops 17696640 | bytes 24336384 | tf_op jit(solution)/shard_map/sub | solution.py:99
  327.9 48.0 %collective-permute-done.3 = bf16[384,1024]{1,0:T(8,128)(2,1)S(1)} collective-permute-done((bf16[384,1024]{1,0:T(8,128)(2,1)}, bf16[384,1024]{1,0:T(8,128)(2,1)S(1)}, u32[]{:S(2)}, u32[]{:S(2)}) %collective-permute-start.3) | collective-permute-done | bytes 786464 | tf_op jit(solution)/shard_map/ppermute | solution.py:15
  382.9 6.3 %copy.31 = bf16[1920,1024]{0,1:T(8,128)(2,1)} copy(bf16[1920,1024]{1,0:T(8,128)(2,1)} %constant_dynamic-update-slice_fusion) | data formatting | bytes 7864320 | tf_op jit(solution)/shard_map/concatenate | solution.py:84
  389.2 8.0 %fusion.13 = f32[4,256,384]{2,1,0:T(8,128)S(1)} fusion(bf16[1920,4,256]{0,2,1:T(8,128)(2,1)} %bitcast.69, f32[4,384,1920]{1,2,0:T(8,128)} %get-tuple-element.16, f32[4,384]{1,0:T(4,128)S(1)} %get-tuple-element.15), kind=kOutput, calls=%fused_computation.19 | convolution fusion | flops 1515847680 | bytes 17307648 | tf_op jit(solution)/shard_map/hqk,khe->qhe/dot_general | solution.py:106
  397.2 6.7 %fusion.24 = (f32[384,4]{0,1:T(4,128)S(1)}, f32[4,256,384]{2,1,0:T(8,128)S(1)}) fusion(f32[4,256,384]{2,1,0:T(8,128)S(1)} %fusion.13, f32[4]{0:T(128)S(1)} %copy-done.19, bf16[1920,4,256]{0,2,1:T(8,128)(2,1)S(1)} %bitcast.70, f32[4,384,1920]{1,2,0:T(8,128)} %get-tuple-element.18, f32[4,384]{1,0:T(4,128)S(1)} %get-tuple-element.17), kind=kOutput, calls=%fused_computation.38 | convolution fusion | flops 1517419008 | bytes 18886672 | tf_op jit(solution)/shard_map/hqk,khe->qhe/dot_general | solution.py:103
  405.0 8.1 %all-gather.6.cloned.1.call-done = bf16[2048,3072]{1,0:T(8,128)(2,1)} async-done(((bf16[256,3072]{1,0:T(8,128)(2,1)}), bf16[2048,3072]{1,0:T(8,128)(2,1)}) %all-gather.6.cloned.1.call-update) | async-done | bytes 12582928 | tf_op jit(solution)/shard_map/all_gather | solution.py:51
  413.4 9.5 %all-gather.10.cloned.1.call-done = bf16[384,2048]{0,1:T(8,128)(2,1)} async-done(((bf16[384,1024]{0,1:T(8,128)(2,1)}), bf16[384,2048]{0,1:T(8,128)(2,1)}) %all-gather.10.cloned.1.call-update) | async-done | bytes 1572880 | tf_op jit(solution)/shard_map/all_gather | solution.py:118
  422.9 4.6 fusion.20
  431.2 28.2 %all-gather.12.cloned.1.call-done = bf16[768,1024]{1,0:T(8,128)(2,1)} async-done(((bf16[384,1024]{1,0:T(8,128)(2,1)}), bf16[768,1024]{1,0:T(8,128)(2,1)}) %all-gather.12.cloned.1.call-update) | async-done | bytes 1572880 | tf_op jit(solution)/shard_map/all_gather | solution.py:132
  459.5 13.7 %all-gather.14.cloned.1.call-done = bf16[768,2048]{1,0:T(8,128)(2,1)} async-done(((bf16[768,1024]{1,0:T(8,128)(2,1)}), bf16[768,2048]{1,0:T(8,128)(2,1)}) %all-gather.14.cloned.1.call-update) | async-done | bytes 3145744 | tf_op jit(solution)/shard_map/all_gather | solution.py:133
  473.2 9.5 %fusion.6 = f32[768,1536]{1,0:T(8,128)} fusion(bf16[768,2048]{1,0:T(8,128)(2,1)} %all-gather.14.cloned.1.call-done, bf16[2048,3072]{1,0:T(8,128)(2,1)} %all-gather.6.cloned.1.call-done), kind=kOutput, calls=%fused_computation.12 | convolution fusion | flops 4831838208 | bytes 14155776 | tf_op jit(solution)/shard_map/dot_general | solution.py:135
  482.7 18.8 %convolution_convert_fusion = bf16[768,2048]{1,0:T(8,128)(2,1)} fusion(bf16[1536,2048]{0,1:T(8,128)(2,1)} %all-gather.8.cloned.1.call-done, f32[768,1536]{1,0:T(8,128)} %fusion.6, bf16[768,2048]{1,0:T(8,128)(2,1)} %all-gather.14.cloned.1.call-done, bf16[2048,3072]{1,0:T(8,128)(2,1)} %all-gather.6.cloned.1.call-done), kind=kOutput, calls=%fused_computation.23 | convolution fusion | flops 9672327168 | bytes 23592960 | tf_op jit(solution)/shard_map/dot_general | solution.py:138
  501.6 12.3 %reduce-scatter.3.cloned.1.call-done = bf16[768,1024]{1,0:T(8,128)(2,1)} async-done(((bf16[768,2048]{1,0:T(8,128)(2,1)}), bf16[768,1024]{1,0:T(8,128)(2,1)}) %reduce-scatter.3.cloned.1.call-update) | async-done | bytes 1572880 | tf_op jit(solution)/shard_map/reduce_scatter | solution.py:139
  514.0 29.3 %reduce-scatter.5.cloned.1.call-done = bf16[384,1024]{1,0:T(8,128)(2,1)} async-done(((bf16[768,1024]{1,0:T(8,128)(2,1)}), bf16[384,1024]{1,0:T(8,128)(2,1)}) %reduce-scatter.5.cloned.1.call-update) | async-done | bytes 786448 | tf_op jit(solution)/shard_map/reduce_scatter | solution.py:143
  (122 shorter events, 63.5 us)
Async XLA Ops:
  6.5 268.9 %copy-start = (bf16[384,512]{1,0:T(8,128)(2,1)S(1)}, bf16[384,512]{1,0:T(8,128)(2,1)}, u32[]{:S(2)}) copy-start(bf16[384,512]{1,0:T(8,128)(2,1)} %param.17) | copy-start | bytes 1179652
  6.5 398.5 %all-gather.8.cloned.1.call-start = ((), (), s32[]{:S(2)}) async-start(), calls=%async_computation.3 | async-start | bytes 7077888 | tf_op jit(solution)/shard_map/all_gather | solution.py:52
  8.5 11.1 %collective-permute-start.17 = (bf16[1,1536,128]{2,1,0:T(8,128)(2,1)}, bf16[1,1536,128]{2,1,0:T(8,128)(2,1)S(1)}, u32[]{:S(2)}, u32[]{:S(2)}) collective-permute-start(bf16[1,1536,128]{2,1,0:T(8,128)(2,1)} %get-tuple-element.13), channel_id=1, source_target_pairs={{0,2},{2,0},{4,6},{6,4},{8,10},{10,8},{12,14},{14,12},{16,18},{18,... | collective-permute-start | bytes 1179656 | tf_op jit(solution)/shard_map/ppermute | solution.py:36
  20.8 392.3 %all-gather.6.cloned.1.call-start = ((), (), s32[]{:S(2)}) async-start(), calls=%async_computation.2 | async-start | bytes 14155776 | tf_op jit(solution)/shard_map/all_gather | solution.py:51
  22.9 18.7 %collective-permute-start.16 = (bf16[1,128,3072]{2,1,0:T(8,128)(2,1)}, bf16[1,128,3072]{2,1,0:T(8,128)(2,1)}, u32[]{:S(2)}, u32[]{:S(2)}) collective-permute-start(bf16[1,128,3072]{2,1,0:T(8,128)(2,1)} %bitcast.10), channel_id=1, source_target_pairs={{0,2},{2,0},{4,6},{6,4},{8,10},{10,8},{12,14},{14,12},{16,18},{18,... | collective-permute-start | bytes 2359304 | tf_op jit(solution)/shard_map/ppermute | solution.py:36
  24.9 30.6 %copy-start.11 = (bf16[384,512]{1,0:T(8,128)(2,1)S(1)}, bf16[384,512]{1,0:T(8,128)(2,1)}, u32[]{:S(2)}) copy-start(bf16[384,512]{1,0:T(8,128)(2,1)} %param.16) | copy-start | bytes 1179652
  44.0 378.9 %all-gather.10.cloned.1.call-start = ((), (), s32[]{:S(2)}) async-start(), calls=%async_computation.4 | async-start | bytes 2359296 | tf_op jit(solution)/shard_map/all_gather | solution.py:118
  45.3 25.1 %collective-permute-start.12 = (bf16[384,512]{0,1:T(8,128)(2,1)S(1)}, bf16[384,512]{0,1:T(8,128)(2,1)S(1)}, u32[]{:S(2)}, u32[]{:S(2)}) collective-permute-start(bf16[384,512]{0,1:T(8,128)(2,1)S(1)} %copy.37), channel_id=1, source_target_pairs={{0,2},{2,4},{4,6},{6,8},{8,10},{10,12},{12,14},{14,16},{16,18},{18... | collective-permute-start | bytes 1179656 | tf_op jit(solution)/shard_map/ppermute | solution.py:15
  48.7 19.8 %collective-permute-start.4 = (s32[384]{0:T(512)S(1)}, s32[384]{0:T(512)S(1)}, u32[]{:S(2)}, u32[]{:S(2)}) collective-permute-start(s32[384]{0:T(512)S(1)} %copy-done.13), channel_id=1, source_target_pairs={{0,2},{2,4},{4,6},{6,8},{8,10},{10,12},{12,14},{14,16},{16,18},{18... | collective-permute-start | bytes 4616 | tf_op jit(solution)/shard_map/ppermute | solution.py:15
  52.1 112.3 %collective-permute-start = (bf16[384,1024]{1,0:T(8,128)(2,1)S(1)}, bf16[384,1024]{1,0:T(8,128)(2,1)S(1)}, u32[]{:S(2)}, u32[]{:S(2)}) collective-permute-start(bf16[384,1024]{1,0:T(8,128)(2,1)S(1)} %copy-done.7), channel_id=1, source_target_pairs={{0,2},{2,4},{4,6},{6,8},{8,10},{10,12},{12,14},{14,16},{16,18},{18... | collective-permute-start | bytes 2359304 | tf_op jit(solution)/shard_map/ppermute | solution.py:15
  55.7 102.8 %collective-permute-start.8 = (bf16[384,512]{0,1:T(8,128)(2,1)S(1)}, bf16[384,512]{0,1:T(8,128)(2,1)S(1)}, u32[]{:S(2)}, u32[]{:S(2)}) collective-permute-start(bf16[384,512]{0,1:T(8,128)(2,1)S(1)} %copy.32), channel_id=1, source_target_pairs={{0,2},{2,4},{4,6},{6,8},{8,10},{10,12},{12,14},{14,16},{16,18},{18... | collective-permute-start | bytes 1179656 | tf_op jit(solution)/shard_map/ppermute | solution.py:15
  68.5 83.7 %copy-start.15 = (s32[384]{0:T(512)}, s32[384]{0:T(512)S(1)}, u32[]{:S(2)}) copy-start(s32[384]{0:T(512)S(1)} %collective-permute-done.4) | copy-start | bytes 4612
  68.5 57.3 %collective-permute-start.5 = (s32[384]{0:T(512)S(1)}, s32[384]{0:T(512)S(1)}, u32[]{:S(2)}, u32[]{:S(2)}) collective-permute-start(s32[384]{0:T(512)S(1)} %collective-permute-done.4), channel_id=1, source_target_pairs={{0,2},{2,4},{4,6},{6,8},{8,10},{10,12},{12,14},{14,16},{16,18},{18... | collective-permute-start | bytes 4616 | tf_op jit(solution)/shard_map/ppermute | solution.py:15
  70.4 90.0 %collective-permute-start.13 = (bf16[384,512]{0,1:T(8,128)(2,1)S(1)}, bf16[384,512]{0,1:T(8,128)(2,1)}, u32[]{:S(2)}, u32[]{:S(2)}) collective-permute-start(bf16[384,512]{0,1:T(8,128)(2,1)S(1)} %collective-permute-done.12), channel_id=1, source_target_pairs={{0,2},{2,4},{4,6},{6,8},{8,10},{10,12},{12,14},{14,16},{16,18},{18... | collective-permute-start | bytes 1179656 | tf_op jit(solution)/shard_map/ppermute | solution.py:15
  125.8 24.4 %collective-permute-start.6 = (s32[384]{0:T(512)S(1)}, s32[384]{0:T(512)}, u32[]{:S(2)}, u32[]{:S(2)}) collective-permute-start(s32[384]{0:T(512)S(1)} %collective-permute-done.5), channel_id=1, source_target_pairs={{0,2},{2,4},{4,6},{6,8},{8,10},{10,12},{12,14},{14,16},{16,18},{18... | collective-permute-start | bytes 4616 | tf_op jit(solution)/shard_map/ppermute | solution.py:15
  150.2 7.6 %collective-permute-start.7 = (s32[384]{0:T(512)}, s32[384]{0:T(512)}, u32[]{:S(2)}, u32[]{:S(2)}) collective-permute-start(s32[384]{0:T(512)} %collective-permute-done.6), channel_id=1, source_target_pairs={{0,2},{2,4},{4,6},{6,8},{8,10},{10,12},{12,14},{14,16},{16,18},{18... | collective-permute-start | bytes 4616 | tf_op jit(solution)/shard_map/ppermute | solution.py:15
  158.5 109.7 %copy-start.12 = (bf16[384,512]{0,1:T(8,128)(2,1)}, bf16[384,512]{0,1:T(8,128)(2,1)S(1)}, u32[]{:S(2)}) copy-start(bf16[384,512]{0,1:T(8,128)(2,1)S(1)} %collective-permute-done.8) | copy-start | bytes 1179652
  158.5 15.7 %collective-permute-start.9 = (bf16[384,512]{0,1:T(8,128)(2,1)S(1)}, bf16[384,512]{0,1:T(8,128)(2,1)S(1)}, u32[]{:S(2)}, u32[]{:S(2)}) collective-permute-start(bf16[384,512]{0,1:T(8,128)(2,1)S(1)} %collective-permute-done.8), channel_id=1, source_target_pairs={{0,2},{2,4},{4,6},{6,8},{8,10},{10,12},{12,14},{14,16},{16,18},{18... | collective-permute-start | bytes 1179656 | tf_op jit(solution)/shard_map/ppermute | solution.py:15
  160.4 34.7 %collective-permute-start.14 = (bf16[384,512]{0,1:T(8,128)(2,1)}, bf16[384,512]{0,1:T(8,128)(2,1)S(1)}, u32[]{:S(2)}, u32[]{:S(2)}) collective-permute-start(bf16[384,512]{0,1:T(8,128)(2,1)} %collective-permute-done.13), channel_id=1, source_target_pairs={{0,2},{2,4},{4,6},{6,8},{8,10},{10,12},{12,14},{14,16},{16,18},{18... | collective-permute-start | bytes 1179656 | tf_op jit(solution)/shard_map/ppermute | solution.py:15
  164.3 103.9 %copy-start.8 = (bf16[384,1024]{1,0:T(8,128)(2,1)}, bf16[384,1024]{1,0:T(8,128)(2,1)S(1)}, u32[]{:S(2)}) copy-start(bf16[384,1024]{1,0:T(8,128)(2,1)S(1)} %collective-permute-done) | copy-start | bytes 2359300
  164.3 100.5 %collective-permute-start.1 = (bf16[384,1024]{1,0:T(8,128)(2,1)S(1)}, bf16[384,1024]{1,0:T(8,128)(2,1)}, u32[]{:S(2)}, u32[]{:S(2)}) collective-permute-start(bf16[384,1024]{1,0:T(8,128)(2,1)S(1)} %collective-permute-done), channel_id=1, source_target_pairs={{0,2},{2,4},{4,6},{6,8},{8,10},{10,12},{12,14},{14,16},{16,18},{18... | collective-permute-start | bytes 2359304 | tf_op jit(solution)/shard_map/ppermute | solution.py:15
  174.2 78.8 %collective-permute-start.10 = (bf16[384,512]{0,1:T(8,128)(2,1)S(1)}, bf16[384,512]{0,1:T(8,128)(2,1)S(1)}, u32[]{:S(2)}, u32[]{:S(2)}) collective-permute-start(bf16[384,512]{0,1:T(8,128)(2,1)S(1)} %collective-permute-done.9), channel_id=1, source_target_pairs={{0,2},{2,4},{4,6},{6,8},{8,10},{10,12},{12,14},{14,16},{16,18},{18... | collective-permute-start | bytes 1179656 | tf_op jit(solution)/shard_map/ppermute | solution.py:15
  195.2 69.6 %collective-permute-start.15 = (bf16[384,512]{0,1:T(8,128)(2,1)S(1)}, bf16[384,512]{0,1:T(8,128)(2,1)S(1)}, u32[]{:S(2)}, u32[]{:S(2)}) collective-permute-start(bf16[384,512]{0,1:T(8,128)(2,1)S(1)} %collective-permute-done.14), channel_id=1, source_target_pairs={{0,2},{2,4},{4,6},{6,8},{8,10},{10,12},{12,14},{14,16},{16,18},{18... | collective-permute-start | bytes 1179656 | tf_op jit(solution)/shard_map/ppermute | solution.py:15
  253.0 22.3 %collective-permute-start.11 = (bf16[384,512]{0,1:T(8,128)(2,1)S(1)}, bf16[384,512]{0,1:T(8,128)(2,1)S(1)}, u32[]{:S(2)}, u32[]{:S(2)}) collective-permute-start(bf16[384,512]{0,1:T(8,128)(2,1)S(1)} %collective-permute-done.10), channel_id=1, source_target_pairs={{0,2},{2,4},{4,6},{6,8},{8,10},{10,12},{12,14},{14,16},{16,18},{18... | collective-permute-start | bytes 1179656 | tf_op jit(solution)/shard_map/ppermute | solution.py:15
  264.9 43.1 %collective-permute-start.2 = (bf16[384,1024]{1,0:T(8,128)(2,1)}, bf16[384,1024]{1,0:T(8,128)(2,1)}, u32[]{:S(2)}, u32[]{:S(2)}) collective-permute-start(bf16[384,1024]{1,0:T(8,128)(2,1)} %collective-permute-done.1), channel_id=1, source_target_pairs={{0,2},{2,4},{4,6},{6,8},{8,10},{10,12},{12,14},{14,16},{16,18},{18... | collective-permute-start | bytes 2359304 | tf_op jit(solution)/shard_map/ppermute | solution.py:15
  308.0 67.8 %collective-permute-start.3 = (bf16[384,1024]{1,0:T(8,128)(2,1)}, bf16[384,1024]{1,0:T(8,128)(2,1)S(1)}, u32[]{:S(2)}, u32[]{:S(2)}) collective-permute-start(bf16[384,1024]{1,0:T(8,128)(2,1)} %collective-permute-done.2), channel_id=1, source_target_pairs={{0,2},{2,4},{4,6},{6,8},{8,10},{10,12},{12,14},{14,16},{16,18},{18... | collective-permute-start | bytes 2359304 | tf_op jit(solution)/shard_map/ppermute | solution.py:15
  327.9 53.1 %copy-start.9 = (bf16[384,1024]{1,0:T(8,128)(2,1)S(1)}, bf16[384,1024]{1,0:T(8,128)(2,1)}, u32[]{:S(2)}) copy-start(bf16[384,1024]{1,0:T(8,128)(2,1)} %copy-done.8) | copy-start | bytes 2359300
  413.1 46.3 %all-gather.12.cloned.1.call-start = ((), (), s32[]{:S(2)}) async-start(), calls=%async_computation.5 | async-start | bytes 2359296 | tf_op jit(solution)/shard_map/all_gather | solution.py:132
  431.2 42.1 %all-gather.14.cloned.1.call-start = ((), (), s32[]{:S(2)}) async-start(), calls=%async_computation.6 | async-start | bytes 4718592 | tf_op jit(solution)/shard_map/all_gather | solution.py:133
  459.4 54.5 %reduce-scatter.3.cloned.1.call-start = ((), (), s32[]{:S(2)}) async-start(), calls=%async_computation.7 | async-start | bytes 4718592 | tf_op jit(solution)/shard_map/reduce_scatter | solution.py:139
  501.5 44.1 %copy-start.1 = (bf16[384,512]{1,0:T(8,128)(2,1)S(1)}, bf16[384,512]{1,0:T(8,128)(2,1)}, u32[]{:S(2)}) copy-start(bf16[384,512]{1,0:T(8,128)(2,1)} %param.17) | copy-start | bytes 1179652
  501.5 41.7 %reduce-scatter.5.cloned.1.call-start = ((), (), s32[]{:S(2)}) async-start(), calls=%async_computation.8 | async-start | bytes 2359296 | tf_op jit(solution)/shard_map/reduce_scatter | solution.py:143
  (13 other events, 183.7 us)
Sparse Core Ops, SparseCore 0:
  20.9 125.1 all-gather.7
  148.3 264.7 all-gather.5
  414.7 8.2 all-gather.9
  431.3 28.0 all-gather.11
  460.8 12.3 all-gather.13
  501.7 12.2 reduce-scatter.2
  516.2 27.0 reduce-scatter.4

commit v3 on v2

--- a/solution.py
+++ b/solution.py
@@ -51,6 +51,32 @@
     both = lax.all_gather(both, "sp", axis=0, tiled=True, axis_index_groups=across)
     down = lax.all_gather(down, "sp", axis=1, tiled=True, axis_index_groups=across)
     return both, down
+
+
+def swapped(value, axis, members):
+    return lax.ppermute(value, axis, [(i, i ^ 1) for i in range(members)])
+
+
+def whole_channels(value):
+    members = lax.axis_size("tp")
+    if members != 2:
+        return lax.all_gather(value, "tp", axis=1, tiled=True)
+    other = swapped(value, "tp", members)
+    mine = lax.axis_index("tp") * value.shape[1]
+    result = jnp.zeros((value.shape[0], 2 * value.shape[1]), value.dtype)
+    result = lax.dynamic_update_slice_in_dim(result, value, mine, 1)
+    return lax.dynamic_update_slice_in_dim(result, other, value.shape[1] - mine, 1)
+
+
+def own_channels(terms):
+    members = lax.axis_size("tp")
+    if members != 2:
+        return lax.psum_scatter(terms, "tp", scatter_dimension=1, tiled=True).astype(jnp.float32)
+    width = terms.shape[1] // 2
+    mine = lax.axis_index("tp") * width
+    other = swapped(lax.dynamic_slice_in_dim(terms, width - mine, width, 1), "tp", members)
+    own = lax.dynamic_slice_in_dim(terms, mine, width, 1)
+    return own.astype(jnp.float32) + other.astype(jnp.float32)
 
 
 def body(
@@ -113,9 +139,8 @@
         .reshape(rows, heads * VD)
         .astype(jnp.bfloat16)
     )
-    attn_rows, both_all, down_all = lax.optimization_barrier((attn_rows, both_all, down_all))
     projected = jnp.dot(
-        lax.all_gather(attn_rows, "tp", axis=1, tiled=True),
+        whole_channels(attn_rows),
         out_weight,
         preferred_element_type=jnp.float32,
     )
@@ -126,24 +151,22 @@
     normed = (midf * lax.rsqrt(squares / channels + 1e-06)[:, None] * mixer_gain).astype(
         jnp.bfloat16
     )
-    plane, across = groups(lax.axis_size("sp"))
-    share = len(plane[0])
-    if share > 1:
-        normed = lax.all_gather(normed, "sp", axis=0, tiled=True, axis_index_groups=plane)
-    whole_rows = lax.all_gather(normed, "tp", axis=1, tiled=True)
+    members = lax.axis_size("sp")
+    paired = len(groups(members)[0][0]) == 2
+    if paired:
+        normed = jnp.concatenate([normed, swapped(normed, "sp", members)], 0)
+    whole_rows = whole_channels(normed)
+    whole_rows, both_all, down_all = lax.optimization_barrier((whole_rows, both_all, down_all))
     part = both_all.shape[1] // 2
     gate = jnp.dot(whole_rows, both_all[:, :part], preferred_element_type=jnp.float32)
     up = jnp.dot(whole_rows, both_all[:, part:], preferred_element_type=jnp.float32)
     hidden = (jax.nn.silu(gate) * up).astype(jnp.bfloat16)
     terms = jnp.dot(hidden, down_all, preferred_element_type=jnp.float32)
-    summed = lax.psum_scatter(
-        terms.astype(jnp.bfloat16), "tp", scatter_dimension=1, tiled=True
-    )
-    if share > 1:
-        summed = lax.psum_scatter(
-            summed, "sp", scatter_dimension=0, tiled=True, axis_index_groups=plane
-        )
-    return (midf + summed.astype(jnp.float32)).astype(jnp.bfloat16)
+    summed = own_channels(terms.astype(jnp.bfloat16))
+    if paired:
+        came = swapped(summed[rows:].astype(jnp.bfloat16), "sp", members)
+        summed = summed[:rows] + came.astype(jnp.float32)
+    return (midf + summed).astype(jnp.bfloat16)
 
 
 def solution(mesh):

time: 560 us -> 502 us (0.90)
  waiting for transfers between devices: 356 us -> 301 us
    all_gather x3 -> x0, waiting for transfers between devices: 51.4 us -> none  [the longest x1 28.2 us: body(): lax.all_gather(normed, 'sp', axis=0, tiled=True, axis_index_groups=plane)]
    ppermute x0 -> x5, waiting for transfers between devices: none -> 47.5 us  [swapped(): return lax.ppermute(value, axis, [(i, i ^ 1) for i in range(members)])]
    reduce_scatter x2 -> x0, waiting for transfers between devices: 41.7 us -> none  [the longest x1 29.3 us: body(): lax.psum_scatter(summed, 'sp', scatter_dimension=0, tiled=True, axis_inde...]
    all_gather x1, waiting for transfers between devices: 8.09 us -> 0.02 us  [gathered(): lax.all_gather(both, 'sp', axis=0, tiled=True, axis_index_groups=across)]
    unnamed x60 -> x68, local copies, waits for them, and re-layouts: 15.4 us -> 15.6 us
  transfers between devices with their start and end apart: 25 -> 25, of which waited for: 18 -> 17; matrix products, arithmetic and copies ran while one was open for 17% -> 20% of each run, Pallas kernels for 0% -> 0%
where the time goes in v3:
time: 502 us; the launch traced here: 497 us
  waiting for transfers between devices  301 us (60%)
  matrix products  56.3 us (11%)
  starting transfers between devices  45.8 us (9%)
  other arithmetic  44.4 us (9%)
  local copies, waits for them, and re-layouts  32 us (6%)
  between operations  14.3 us (3%)
    ppermute x16, waiting for transfers between devices, shifted(): return lax.ppermute(value, axis, pairs)  228 us
    ppermute x5, waiting for transfers between devices, swapped(): return lax.ppermute(value, axis, [(i, i ^ 1) for i in range(members)])  47.5 us
    ppermute x16, starting transfers between devices, shifted(): return lax.ppermute(value, axis, pairs)  42 us
    sub x2, other arithmetic, weights(): score = score - jnp.max(score, axis=-1, keepdims=True)  36.7 us
    ppermute x2, waiting for transfers between devices, spread(): came = lax.ppermute(sent, 'sp', pairs)  26 us
    dot_general x1, matrix products, body(): terms = jnp.dot(hidden, down_all, preferred_element_type=jnp.float32)  17.8 us
    unnamed x68, local copies, waits for them, and re-layouts  15.6 us
    dot_general x2, matrix products, weights(): jnp.einsum('qhd,khd->hqk', query.reshape(rows, heads, HD), keys, preferre...  12.4 us
  transfers between devices with their start and end apart: 25, of which 17 were waited for; matrix products, arithmetic and copies ran while one was open for 20% of the time, Pallas kernels for 0%

profile of v3, /device:TPU:16, one launch (start us, length us, event | category | flops | bytes accessed | tf_op | source)
XLA Modules:
  0.0 496.8 jit_solution(3711081791388752364)
XLA Ops:
  10.3 9.3 %collective-permute-done.20 = bf16[1,1536,128]{2,1,0:T(8,128)(2,1)S(1)} collective-permute-done((bf16[1,1536,128]{2,1,0:T(8,128)(2,1)}, bf16[1,1536,128]{2,1,0:T(8,128)(2,1)S(1)}, u32[]{:S(2)}, u32[]{:S(2)}) %collective-permute-start.20) | collective-permute-done | bytes 393248 | tf_op jit(solution)/shard_map/ppermute | solution.py:36
  25.0 16.7 %collective-permute-done.19 = bf16[1,128,3072]{2,1,0:T(8,128)(2,1)} collective-permute-done((bf16[1,128,3072]{2,1,0:T(8,128)(2,1)}, bf16[1,128,3072]{2,1,0:T(8,128)(2,1)}, u32[]{:S(2)}, u32[]{:S(2)}) %collective-permute-start.19) | collective-permute-done | bytes 786464 | tf_op jit(solution)/shard_map/ppermute | solution.py:36
  45.2 3.4 collective-permute-start.12
  48.6 3.4 collective-permute-start.4
  52.1 3.4 collective-permute-start
  55.7 3.4 collective-permute-start.8
  59.1 9.4 %collective-permute-done.4 = s32[384]{0:T(512)S(1)} collective-permute-done((s32[384]{0:T(512)S(1)}, s32[384]{0:T(512)S(1)}, u32[]{:S(2)}, u32[]{:S(2)}) %collective-permute-start.4) | collective-permute-done | bytes 1568 | tf_op jit(solution)/shard_map/ppermute | solution.py:15
  72.4 53.3 %collective-permute-done.5 = s32[384]{0:T(512)S(1)} collective-permute-done((s32[384]{0:T(512)S(1)}, s32[384]{0:T(512)S(1)}, u32[]{:S(2)}, u32[]{:S(2)}) %collective-permute-start.5) | collective-permute-done | bytes 1568 | tf_op jit(solution)/shard_map/ppermute | solution.py:15
  128.3 22.0 %collective-permute-done.6 = s32[384]{0:T(512)} collective-permute-done((s32[384]{0:T(512)S(1)}, s32[384]{0:T(512)}, u32[]{:S(2)}, u32[]{:S(2)}) %collective-permute-start.6) | collective-permute-done | bytes 1568 | tf_op jit(solution)/shard_map/ppermute | solution.py:15
  152.8 5.1 %collective-permute-done.7 = s32[384]{0:T(512)} collective-permute-done((s32[384]{0:T(512)}, s32[384]{0:T(512)}, u32[]{:S(2)}, u32[]{:S(2)}) %collective-permute-start.7) | collective-permute-done | bytes 1568 | tf_op jit(solution)/shard_map/ppermute | solution.py:15
  164.4 5.7 %collective-permute-start.1 = (bf16[384,1024]{1,0:T(8,128)(2,1)S(1)}, bf16[384,1024]{1,0:T(8,128)(2,1)}, u32[]{:S(2)}, u32[]{:S(2)}) collective-permute-start(bf16[384,1024]{1,0:T(8,128)(2,1)S(1)} %collective-permute-done), channel_id=1, source_target_pairs={{0,2},{2,4},{4,6},{6,8},{8,10},{10,12},{12,14},{14,16},{16,18},{18... | collective-permute-start | bytes 2359304 | tf_op jit(solution)/shard_map/ppermute | solution.py:15
  170.8 3.4 collective-permute-done.9
  174.2 2.7 collective-permute-start.10
  176.9 18.0 %collective-permute-done.14 = bf16[384,512]{0,1:T(8,128)(2,1)S(1)} collective-permute-done((bf16[384,512]{0,1:T(8,128)(2,1)S(1)}, bf16[384,512]{0,1:T(8,128)(2,1)S(1)}, u32[]{:S(2)}, u32[]{:S(2)}) %collective-permute-start.14) | collective-permute-done | bytes 393248 | tf_op jit(solution)/shard_map/ppermute | solution.py:15
  196.9 3.7 and_and_fusion
  200.6 52.3 %collective-permute-done.10 = bf16[384,512]{0,1:T(8,128)(2,1)S(1)} collective-permute-done((bf16[384,512]{0,1:T(8,128)(2,1)S(1)}, bf16[384,512]{0,1:T(8,128)(2,1)S(1)}, u32[]{:S(2)}, u32[]{:S(2)}) %collective-permute-start.10) | collective-permute-done | bytes 393248 | tf_op jit(solution)/shard_map/ppermute | solution.py:15
  254.8 9.9 %collective-permute-done.15 = bf16[384,512]{0,1:T(8,128)(2,1)S(1)} collective-permute-done((bf16[384,512]{0,1:T(8,128)(2,1)S(1)}, bf16[384,512]{0,1:T(8,128)(2,1)S(1)}, u32[]{:S(2)}, u32[]{:S(2)}) %collective-permute-start.15) | collective-permute-done | bytes 393248 | tf_op jit(solution)/shard_map/ppermute | solution.py:15
  268.3 7.0 %collective-permute-done.11 = bf16[384,512]{0,1:T(8,128)(2,1)S(1)} collective-permute-done((bf16[384,512]{0,1:T(8,128)(2,1)S(1)}, bf16[384,512]{0,1:T(8,128)(2,1)S(1)}, u32[]{:S(2)}, u32[]{:S(2)}) %collective-permute-start.11) | collective-permute-done | bytes 393248 | tf_op jit(solution)/shard_map/ppermute | solution.py:15
  275.5 6.2 %fusion.29 = f32[4,1920,384]{2,1,0:T(8,128)} fusion(bf16[1920,4,128]{0,2,1:T(8,128)(2,1)S(1)} %bitcast.76, bf16[384,512]{1,0:T(8,128)(2,1)S(1)} %copy-done), kind=kOutput, calls=%fused_computation.50 | convolution fusion | flops 754974720 | bytes 14155776 | tf_op jit(solution)/shard_map/qhd,khd->hqk/dot_general | solution.py:121
  281.7 19.0 %fusion.40 = (f32[4,384]{1,0:T(4,128)S(1)}, f32[4,384,1920]{1,2,0:T(8,128)}) fusion(f32[4,1920,384]{2,1,0:T(8,128)} %fusion.29, pred[384,1920]{0,1:T(8,128)(4,1)} %and_and_fusion), kind=kOutput, calls=%fused_computation.96 | output fusion | flops 17696640 | bytes 24336384 | tf_op jit(solution)/shard_map/sub | solution.py:125
  301.8 6.2 %fusion.32 = f32[4,1920,384]{2,1,0:T(8,128)} fusion(bf16[1920,4,128]{0,2,1:T(8,128)(2,1)S(1)} %bitcast.77, bf16[384,512]{1,0:T(8,128)(2,1)S(1)} %copy-done.13), kind=kOutput, calls=%fused_computation.53 | convolution fusion | flops 754974720 | bytes 14155776 | tf_op jit(solution)/shard_map/qhd,khd->hqk/dot_general | solution.py:121
  310.4 17.8 %fusion.41 = (f32[4,384]{1,0:T(4,128)S(1)}, f32[4,384,1920]{1,2,0:T(8,128)}) fusion(f32[4,1920,384]{2,1,0:T(8,128)} %fusion.32, pred[384,1920]{0,1:T(8,128)(4,1)} %and_and_fusion), kind=kOutput, calls=%fused_computation.97 | output fusion | flops 17696640 | bytes 24336384 | tf_op jit(solution)/shard_map/sub | solution.py:125
  328.2 47.6 %collective-permute-done.3 = bf16[384,1024]{1,0:T(8,128)(2,1)S(1)} collective-permute-done((bf16[384,1024]{1,0:T(8,128)(2,1)}, bf16[384,1024]{1,0:T(8,128)(2,1)S(1)}, u32[]{:S(2)}, u32[]{:S(2)}) %collective-permute-start.3) | collective-permute-done | bytes 786464 | tf_op jit(solution)/shard_map/ppermute | solution.py:15
  382.8 6.4 %copy.31 = bf16[1920,1024]{0,1:T(8,128)(2,1)} copy(bf16[1920,1024]{1,0:T(8,128)(2,1)} %constant_dynamic-update-slice_fusion) | data formatting | bytes 7864320 | tf_op jit(solution)/shard_map/concatenate | solution.py:110
  389.2 8.0 %fusion.13 = f32[4,256,384]{2,1,0:T(8,128)S(1)} fusion(bf16[1920,4,256]{0,2,1:T(8,128)(2,1)} %bitcast.69, f32[4,384,1920]{1,2,0:T(8,128)} %get-tuple-element.18, f32[4,384]{1,0:T(4,128)S(1)} %get-tuple-element.17), kind=kOutput, calls=%fused_computation.19 | convolution fusion | flops 1515847680 | bytes 17307648 | tf_op jit(solution)/shard_map/hqk,khe->qhe/dot_general | solution.py:132
  397.2 6.7 %fusion.24 = (f32[384,4]{0,1:T(4,128)S(1)}, f32[4,256,384]{2,1,0:T(8,128)S(1)}) fusion(f32[4,256,384]{2,1,0:T(8,128)S(1)} %fusion.13, f32[4]{0:T(128)S(1)} %copy-done.23, bf16[1920,4,256]{0,2,1:T(8,128)(2,1)S(1)} %bitcast.70, f32[4,384,1920]{1,2,0:T(8,128)} %get-tuple-element.20, f32[4,384]{1,0:T(4,128)S(1)} %get-tuple-element.19), kind=kOutput, calls=%fused_computation.42 | convolution fusion | flops 1517419008 | bytes 18886672 | tf_op jit(solution)/shard_map/hqk,khe->qhe/dot_general | solution.py:129
  411.5 19.6 %collective-permute-done.17 = bf16[384,1024]{1,0:T(8,128)(2,1)S(1)} collective-permute-done((bf16[384,1024]{1,0:T(8,128)(2,1)S(1)}, bf16[384,1024]{1,0:T(8,128)(2,1)S(1)}, u32[]{:S(2)}, u32[]{:S(2)}) %collective-permute-start.17) | collective-permute-done | bytes 786464 | tf_op jit(solution)/shard_map/ppermute | solution.py:57
  431.9 3.4 collective-permute-done.18
  435.5 9.6 %fusion.6 = f32[768,1536]{1,0:T(8,128)} fusion(bf16[768,2048]{1,0:T(8,128)(2,1)S(1)} %constant_dynamic-update-slice_fusion.23, bf16[2048,3072]{1,0:T(8,128)(2,1)} %all-gather.3.cloned.1.call-done), kind=kOutput, calls=%fused_computation.12 | convolution fusion | flops 4831838208 | bytes 14155776 | tf_op jit(solution)/shard_map/dot_general | solution.py:161
  445.1 17.8 %convolution_convert_fusion = bf16[768,2048]{1,0:T(8,128)(2,1)} fusion(bf16[1536,2048]{0,1:T(8,128)(2,1)} %all-gather.5.cloned.1.call-done, f32[768,1536]{1,0:T(8,128)} %fusion.6, bf16[768,2048]{1,0:T(8,128)(2,1)S(1)} %constant_dynamic-update-slice_fusion.23, bf16[2048,3072]{1,0:T(8,128)(2,1)} %all-gather.3.cloned.1.call-done), kind=kOutput, calls=%fused_computation.23 | convolution fusion | flops 9672327168 | bytes 23592960 | tf_op jit(solution)/shard_map/dot_general | solution.py:164
  464.8 3.3 collective-permute-done.21
  469.2 19.3 %collective-permute-done.22 = bf16[384,1024]{1,0:T(8,128)(2,1)S(1)} collective-permute-done((bf16[384,1024]{1,0:T(8,128)(2,1)S(1)}, bf16[384,1024]{1,0:T(8,128)(2,1)S(1)}, u32[]{:S(2)}, u32[]{:S(2)}) %collective-permute-start.22) | collective-permute-done | bytes 786464 | tf_op jit(solution)/shard_map/ppermute | solution.py:57
  (134 shorter events, 59.7 us)
Async XLA Ops:
  6.5 269.0 %copy-start = (bf16[384,512]{1,0:T(8,128)(2,1)S(1)}, bf16[384,512]{1,0:T(8,128)(2,1)}, u32[]{:S(2)}) copy-start(bf16[384,512]{1,0:T(8,128)(2,1)} %param.17) | copy-start | bytes 1179652
  6.5 428.9 %all-gather.5.cloned.1.call-start = ((), (), s32[]{:S(2)}) async-start(), calls=%async_computation.1 | async-start | bytes 7077888 | tf_op jit(solution)/shard_map/all_gather | solution.py:52
  8.5 11.1 %collective-permute-start.20 = (bf16[1,1536,128]{2,1,0:T(8,128)(2,1)}, bf16[1,1536,128]{2,1,0:T(8,128)(2,1)S(1)}, u32[]{:S(2)}, u32[]{:S(2)}) collective-permute-start(bf16[1,1536,128]{2,1,0:T(8,128)(2,1)} %get-tuple-element.15), channel_id=1, source_target_pairs={{0,2},{2,0},{4,6},{6,4},{8,10},{10,8},{12,14},{14,12},{16,18},{18,... | collective-permute-start | bytes 1179656 | tf_op jit(solution)/shard_map/ppermute | solution.py:36
  20.8 414.7 %all-gather.3.cloned.1.call-start = ((), (), s32[]{:S(2)}) async-start(), calls=%async_computation | async-start | bytes 14155776 | tf_op jit(solution)/shard_map/all_gather | solution.py:51
  22.9 18.7 %collective-permute-start.19 = (bf16[1,128,3072]{2,1,0:T(8,128)(2,1)}, bf16[1,128,3072]{2,1,0:T(8,128)(2,1)}, u32[]{:S(2)}, u32[]{:S(2)}) collective-permute-start(bf16[1,128,3072]{2,1,0:T(8,128)(2,1)} %bitcast.10), channel_id=1, source_target_pairs={{0,2},{2,0},{4,6},{6,4},{8,10},{10,8},{12,14},{14,12},{16,18},{18,... | collective-permute-start | bytes 2359304 | tf_op jit(solution)/shard_map/ppermute | solution.py:36
  24.9 27.2 %copy-start.10 = (bf16[384,1024]{1,0:T(8,128)(2,1)S(1)}, bf16[384,1024]{1,0:T(8,128)(2,1)}, u32[]{:S(2)}) copy-start(bf16[384,1024]{1,0:T(8,128)(2,1)} %param.19) | copy-start | bytes 2359300
  24.9 30.5 %copy-start.14 = (bf16[384,512]{1,0:T(8,128)(2,1)S(1)}, bf16[384,512]{1,0:T(8,128)(2,1)}, u32[]{:S(2)}) copy-start(bf16[384,512]{1,0:T(8,128)(2,1)} %param.16) | copy-start | bytes 1179652
  45.2 25.3 %collective-permute-start.12 = (bf16[384,512]{0,1:T(8,128)(2,1)S(1)}, bf16[384,512]{0,1:T(8,128)(2,1)}, u32[]{:S(2)}, u32[]{:S(2)}) collective-permute-start(bf16[384,512]{0,1:T(8,128)(2,1)S(1)} %copy.37), channel_id=1, source_target_pairs={{0,2},{2,4},{4,6},{6,8},{8,10},{10,12},{12,14},{14,16},{16,18},{18... | collective-permute-start | bytes 1179656 | tf_op jit(solution)/shard_map/ppermute | solution.py:15
  48.6 19.9 %collective-permute-start.4 = (s32[384]{0:T(512)S(1)}, s32[384]{0:T(512)S(1)}, u32[]{:S(2)}, u32[]{:S(2)}) collective-permute-start(s32[384]{0:T(512)S(1)} %copy-done.16), channel_id=1, source_target_pairs={{0,2},{2,4},{4,6},{6,8},{8,10},{10,12},{12,14},{14,16},{16,18},{18... | collective-permute-start | bytes 4616 | tf_op jit(solution)/shard_map/ppermute | solution.py:15
  52.1 112.4 %collective-permute-start = (bf16[384,1024]{1,0:T(8,128)(2,1)S(1)}, bf16[384,1024]{1,0:T(8,128)(2,1)S(1)}, u32[]{:S(2)}, u32[]{:S(2)}) collective-permute-start(bf16[384,1024]{1,0:T(8,128)(2,1)S(1)} %copy-done.10), channel_id=1, source_target_pairs={{0,2},{2,4},{4,6},{6,8},{8,10},{10,12},{12,14},{14,16},{16,18},{18... | collective-permute-start | bytes 2359304 | tf_op jit(solution)/shard_map/ppermute | solution.py:15
  55.7 102.8 %collective-permute-start.8 = (bf16[384,512]{0,1:T(8,128)(2,1)S(1)}, bf16[384,512]{0,1:T(8,128)(2,1)S(1)}, u32[]{:S(2)}, u32[]{:S(2)}) collective-permute-start(bf16[384,512]{0,1:T(8,128)(2,1)S(1)} %copy.32), channel_id=1, source_target_pairs={{0,2},{2,4},{4,6},{6,8},{8,10},{10,12},{12,14},{14,16},{16,18},{18... | collective-permute-start | bytes 1179656 | tf_op jit(solution)/shard_map/ppermute | solution.py:15
  68.6 83.6 %copy-start.18 = (s32[384]{0:T(512)}, s32[384]{0:T(512)S(1)}, u32[]{:S(2)}) copy-start(s32[384]{0:T(512)S(1)} %collective-permute-done.4) | copy-start | bytes 4612
  68.6 57.2 %collective-permute-start.5 = (s32[384]{0:T(512)S(1)}, s32[384]{0:T(512)S(1)}, u32[]{:S(2)}, u32[]{:S(2)}) collective-permute-start(s32[384]{0:T(512)S(1)} %collective-permute-done.4), channel_id=1, source_target_pairs={{0,2},{2,4},{4,6},{6,8},{8,10},{10,12},{12,14},{14,16},{16,18},{18... | collective-permute-start | bytes 4616 | tf_op jit(solution)/shard_map/ppermute | solution.py:15
  70.5 89.9 %collective-permute-start.13 = (bf16[384,512]{0,1:T(8,128)(2,1)}, bf16[384,512]{0,1:T(8,128)(2,1)S(1)}, u32[]{:S(2)}, u32[]{:S(2)}) collective-permute-start(bf16[384,512]{0,1:T(8,128)(2,1)} %collective-permute-done.12), channel_id=1, source_target_pairs={{0,2},{2,4},{4,6},{6,8},{8,10},{10,12},{12,14},{14,16},{16,18},{18... | collective-permute-start | bytes 1179656 | tf_op jit(solution)/shard_map/ppermute | solution.py:15
  125.8 24.5 %collective-permute-start.6 = (s32[384]{0:T(512)S(1)}, s32[384]{0:T(512)}, u32[]{:S(2)}, u32[]{:S(2)}) collective-permute-start(s32[384]{0:T(512)S(1)} %collective-permute-done.5), channel_id=1, source_target_pairs={{0,2},{2,4},{4,6},{6,8},{8,10},{10,12},{12,14},{14,16},{16,18},{18... | collective-permute-start | bytes 4616 | tf_op jit(solution)/shard_map/ppermute | solution.py:15
  150.2 7.6 %collective-permute-start.7 = (s32[384]{0:T(512)}, s32[384]{0:T(512)}, u32[]{:S(2)}, u32[]{:S(2)}) collective-permute-start(s32[384]{0:T(512)} %collective-permute-done.6), channel_id=1, source_target_pairs={{0,2},{2,4},{4,6},{6,8},{8,10},{10,12},{12,14},{14,16},{16,18},{18... | collective-permute-start | bytes 4616 | tf_op jit(solution)/shard_map/ppermute | solution.py:15
  158.5 109.8 %copy-start.15 = (bf16[384,512]{0,1:T(8,128)(2,1)}, bf16[384,512]{0,1:T(8,128)(2,1)S(1)}, u32[]{:S(2)}) copy-start(bf16[384,512]{0,1:T(8,128)(2,1)S(1)} %collective-permute-done.8) | copy-start | bytes 1179652
  158.5 15.7 %collective-permute-start.9 = (bf16[384,512]{0,1:T(8,128)(2,1)S(1)}, bf16[384,512]{0,1:T(8,128)(2,1)S(1)}, u32[]{:S(2)}, u32[]{:S(2)}) collective-permute-start(bf16[384,512]{0,1:T(8,128)(2,1)S(1)} %collective-permute-done.8), channel_id=1, source_target_pairs={{0,2},{2,4},{4,6},{6,8},{8,10},{10,12},{12,14},{14,16},{16,18},{18... | collective-permute-start | bytes 1179656 | tf_op jit(solution)/shard_map/ppermute | solution.py:15
  160.4 34.5 %collective-permute-start.14 = (bf16[384,512]{0,1:T(8,128)(2,1)S(1)}, bf16[384,512]{0,1:T(8,128)(2,1)S(1)}, u32[]{:S(2)}, u32[]{:S(2)}) collective-permute-start(bf16[384,512]{0,1:T(8,128)(2,1)S(1)} %collective-permute-done.13), channel_id=1, source_target_pairs={{0,2},{2,4},{4,6},{6,8},{8,10},{10,12},{12,14},{14,16},{16,18},{18... | collective-permute-start | bytes 1179656 | tf_op jit(solution)/shard_map/ppermute | solution.py:15
  164.4 103.9 %copy-start.11 = (bf16[384,1024]{1,0:T(8,128)(2,1)}, bf16[384,1024]{1,0:T(8,128)(2,1)S(1)}, u32[]{:S(2)}) copy-start(bf16[384,1024]{1,0:T(8,128)(2,1)S(1)} %collective-permute-done) | copy-start | bytes 2359300
  164.4 100.4 %collective-permute-start.1 = (bf16[384,1024]{1,0:T(8,128)(2,1)S(1)}, bf16[384,1024]{1,0:T(8,128)(2,1)}, u32[]{:S(2)}, u32[]{:S(2)}) collective-permute-start(bf16[384,1024]{1,0:T(8,128)(2,1)S(1)} %collective-permute-done), channel_id=1, source_target_pairs={{0,2},{2,4},{4,6},{6,8},{8,10},{10,12},{12,14},{14,16},{16,18},{18... | collective-permute-start | bytes 2359304 | tf_op jit(solution)/shard_map/ppermute | solution.py:15
  174.2 78.7 %collective-permute-start.10 = (bf16[384,512]{0,1:T(8,128)(2,1)S(1)}, bf16[384,512]{0,1:T(8,128)(2,1)S(1)}, u32[]{:S(2)}, u32[]{:S(2)}) collective-permute-start(bf16[384,512]{0,1:T(8,128)(2,1)S(1)} %collective-permute-done.9), channel_id=1, source_target_pairs={{0,2},{2,4},{4,6},{6,8},{8,10},{10,12},{12,14},{14,16},{16,18},{18... | collective-permute-start | bytes 1179656 | tf_op jit(solution)/shard_map/ppermute | solution.py:15
  194.9 69.8 %collective-permute-start.15 = (bf16[384,512]{0,1:T(8,128)(2,1)S(1)}, bf16[384,512]{0,1:T(8,128)(2,1)S(1)}, u32[]{:S(2)}, u32[]{:S(2)}) collective-permute-start(bf16[384,512]{0,1:T(8,128)(2,1)S(1)} %collective-permute-done.14), channel_id=1, source_target_pairs={{0,2},{2,4},{4,6},{6,8},{8,10},{10,12},{12,14},{14,16},{16,18},{18... | collective-permute-start | bytes 1179656 | tf_op jit(solution)/shard_map/ppermute | solution.py:15
  252.9 22.4 %collective-permute-start.11 = (bf16[384,512]{0,1:T(8,128)(2,1)S(1)}, bf16[384,512]{0,1:T(8,128)(2,1)S(1)}, u32[]{:S(2)}, u32[]{:S(2)}) collective-permute-start(bf16[384,512]{0,1:T(8,128)(2,1)S(1)} %collective-permute-done.10), channel_id=1, source_target_pairs={{0,2},{2,4},{4,6},{6,8},{8,10},{10,12},{12,14},{14,16},{16,18},{18... | collective-permute-start | bytes 1179656 | tf_op jit(solution)/shard_map/ppermute | solution.py:15
  264.9 43.1 %collective-permute-start.2 = (bf16[384,1024]{1,0:T(8,128)(2,1)}, bf16[384,1024]{1,0:T(8,128)(2,1)}, u32[]{:S(2)}, u32[]{:S(2)}) collective-permute-start(bf16[384,1024]{1,0:T(8,128)(2,1)} %collective-permute-done.1), channel_id=1, source_target_pairs={{0,2},{2,4},{4,6},{6,8},{8,10},{10,12},{12,14},{14,16},{16,18},{18... | collective-permute-start | bytes 2359304 | tf_op jit(solution)/shard_map/ppermute | solution.py:15
  308.0 67.8 %collective-permute-start.3 = (bf16[384,1024]{1,0:T(8,128)(2,1)}, bf16[384,1024]{1,0:T(8,128)(2,1)S(1)}, u32[]{:S(2)}, u32[]{:S(2)}) collective-permute-start(bf16[384,1024]{1,0:T(8,128)(2,1)} %collective-permute-done.2), channel_id=1, source_target_pairs={{0,2},{2,4},{4,6},{6,8},{8,10},{10,12},{12,14},{14,16},{16,18},{18... | collective-permute-start | bytes 2359304 | tf_op jit(solution)/shard_map/ppermute | solution.py:15
  328.2 52.7 %copy-start.12 = (bf16[384,1024]{1,0:T(8,128)(2,1)S(1)}, bf16[384,1024]{1,0:T(8,128)(2,1)}, u32[]{:S(2)}) copy-start(bf16[384,1024]{1,0:T(8,128)(2,1)} %copy-done.11) | copy-start | bytes 2359300
  404.2 2.4 collective-permute-start.16
  411.4 19.7 %collective-permute-start.17 = (bf16[384,1024]{1,0:T(8,128)(2,1)S(1)}, bf16[384,1024]{1,0:T(8,128)(2,1)S(1)}, u32[]{:S(2)}, u32[]{:S(2)}) collective-permute-start(bf16[384,1024]{1,0:T(8,128)(2,1)S(1)} %fusion.22), channel_id=1, source_target_pairs={{0,2},{2,0},{4,6},{6,4},{8,10},{10,8},{12,14},{14,12},{16,18},{18,... | collective-permute-start | bytes 2359304 | tf_op jit(solution)/shard_map/ppermute | solution.py:57
  431.8 3.5 collective-permute-start.18
  464.6 3.5 collective-permute-start.21
  468.9 19.6 %collective-permute-start.22 = (bf16[384,1024]{1,0:T(8,128)(2,1)S(1)}, bf16[384,1024]{1,0:T(8,128)(2,1)S(1)}, u32[]{:S(2)}, u32[]{:S(2)}) collective-permute-start(bf16[384,1024]{1,0:T(8,128)(2,1)S(1)} %slice.31), channel_id=1, source_target_pairs={{0,2},{2,0},{4,6},{6,4},{8,10},{10,8},{12,14},{14,12},{16,18},{18,... | collective-permute-start | bytes 2359304 | tf_op jit(solution)/shard_map/ppermute | solution.py:57
  (17 other events, 183.7 us)
Sparse Core Ops, SparseCore 0:
  20.9 125.2 all-gather.4
  148.4 264.6 all-gather.2
